TPU v7x, 256 devices: a whole 4x4x8 slice. The times are simulated.
256 devices in a mesh: ep: 64 (over z, y, core), tp: 4 (over x).
Axes of the slice: x: 4, y: 4, z: 8, core: 2. Of those that a mesh axis runs over, the one named last changes fastest.
Arguments:
- q_heads: bfloat16 [65536, 1024], P('ep', 'tp'), may hold values from -200 to 200
- k_heads: bfloat16 [65536, 256], P('ep', 'tp'), may hold values from -6 to 6
- v_heads: bfloat16 [65536, 256], P('ep', 'tp'), may hold values from -6 to 6
- sink_logits: float32 [16], P('tp'), may hold values from 1 to 5
- out_weight: bfloat16 [1024, 2048], P(None, 'tp'), may hold values from -1.5 to 1.5
- tokens_b: bfloat16 [32768, 2048], P('ep'), may hold values from -6 to 6
- moe_gain: float32 [2048], replicated, may hold values from 0.1 to 1.9
- router_group: bfloat16 [2048, 4], replicated, may hold values from -0.125 to 0.125
- router_expert: bfloat16 [2048, 128], replicated, may hold values from -0.125 to 0.125
- route_expert: int32 [32768, 2], P('ep'), may hold values from 0 to 127, as said below
- expert_gate: bfloat16 [128, 2048, 1024], P('ep', None, 'tp'), may hold values from -0.125 to 0.125
- expert_up: bfloat16 [128, 2048, 1024], P('ep', None, 'tp'), may hold values from -0.125 to 0.125
- expert_down: bfloat16 [128, 1024, 2048], P('ep', 'tp'), may hold values from -0.75 to 0.75
Outputs:
- mixer_out: bfloat16 [65536, 2048], P('ep', 'tp')
- moe_out: bfloat16 [32768, 2048], P(('ep', 'tp'))
Inputs may be any that keep to these rules, and one draw needn't show every extreme that they name: `route_expert`: each token names two different experts, in rising order, of one group of 32 consecutive experts. In each aligned block of 128 rows (the rows of one device) no expert is named by more than 4 tokens, in each group one expert is named by exactly 4 tokens of every block, and each group is named by a quarter of every block's tokens.
All inputs are finite; a program needn't handle non-finite values.
Results may differ from a plain program's by a relative error of at most 0.011.
Values may be sent and summed in bfloat16 or wider, within the bound.
A program may use at most 128 MiB of HBM per device.

v0:
```python
import jax
import jax.numpy as jnp
from jax import lax
from jax.sharding import PartitionSpec as P

HEADS = 16
KV = 4
HD = 64
WINDOW = 128


def shifted(value, axis, steps):
    count = lax.axis_size(axis)
    leading, last = (max(0, -steps), min(count, count - steps))
    return lax.ppermute(value, axis, [(source, source + steps) for source in range(leading, last)])


def in_blocks(array, dim, peers):
    before, after = (array.shape[:dim], array.shape[dim + 1 :])
    return jnp.moveaxis(array.reshape(*before, peers, -1, *after), dim, 0)


def summed_on_arrival(array, axis, dim):
    peers = lax.axis_size(axis)
    parts = lax.all_to_all(in_blocks(array, dim, peers), axis, 0, 0, tiled=True)
    return jnp.sum(parts.astype(jnp.float32), axis=0)


def normalize(rows_in, gain):
    values = rows_in.astype(jnp.float32)
    scaled = values * lax.rsqrt(jnp.mean(values * values, axis=-1, keepdims=True) + 1e-06) * gain
    return scaled.astype(jnp.bfloat16)


def gate_weights(normed, routes, router_group, router_expert):
    group_logits = jnp.dot(normed, router_group, preferred_element_type=jnp.float32)
    expert_logits = jnp.dot(normed, router_expert, preferred_element_type=jnp.float32)
    group_count = router_group.shape[1]
    expert_count = router_expert.shape[1]
    chosen_group = routes[:, 0] // (expert_count // group_count)
    group_match = chosen_group[:, None] == jnp.arange(group_count, dtype=jnp.int32)[None, :]
    group_share = jnp.sum(
        jnp.where(group_match, jax.nn.softmax(group_logits, axis=-1), 0.0), axis=-1
    )
    expert_match = routes[:, :, None] == jnp.arange(expert_count, dtype=jnp.int32)[None, None, :]
    picked = jnp.sum(jnp.where(expert_match, expert_logits[:, None, :], 0.0), axis=-1)
    return group_share[:, None] * jax.nn.softmax(picked, axis=-1)


def slot_positions(routes, sub_count, expert_count):
    flat_routes = routes.reshape(sub_count, -1)
    onehot = (
        flat_routes[:, :, None] == jnp.arange(expert_count, dtype=jnp.int32)[None, None, :]
    ).astype(jnp.int32)
    places = jnp.sum(onehot * jnp.cumsum(onehot, axis=1), axis=2) - 1
    return (flat_routes, places)


def fill_slots(normed, flat_routes, places, sub_count, expert_count, capacity, exp_local):
    sub_index = jnp.arange(sub_count, dtype=jnp.int32)[:, None]
    target = ((flat_routes * sub_count + sub_index) * capacity + places).reshape(-1)
    source = jnp.repeat(normed, 2, axis=0)
    buffer = jnp.zeros((expert_count * sub_count * capacity, normed.shape[1]), jnp.bfloat16)
    buffer = buffer.at[target].set(source)
    return buffer.reshape(
        expert_count // exp_local, exp_local, sub_count, capacity, normed.shape[1]
    )


def per_device(
    q_heads,
    k_heads,
    v_heads,
    sink_logits,
    out_weight,
    tokens_b,
    moe_gain,
    router_group,
    router_expert,
    route_expert,
    expert_gate,
    expert_up,
    expert_down,
):
    span_len = WINDOW
    row_count = q_heads.shape[0]
    kv_local = k_heads.shape[1] // HD
    group_size = HEADS // KV
    blocks = row_count // span_len
    stacked = jnp.stack([k_heads[row_count - span_len :], v_heads[row_count - span_len :]])
    earlier = shifted(stacked, "ep", 1)

    def make_band(own_rows, prev_rows):
        extended = jnp.concatenate([prev_rows, own_rows], axis=0).reshape(
            blocks + 1, span_len, kv_local, HD
        )
        return jnp.concatenate([extended[:-1], extended[1:]], axis=1)

    key_band = make_band(k_heads, earlier[0])
    value_band = make_band(v_heads, earlier[1])
    query_blocks = q_heads.reshape(blocks, span_len, kv_local, group_size, HD)
    scores = jnp.einsum(
        "nqhgd,nkhd->nhgqk", query_blocks, key_band, preferred_element_type=jnp.float32
    ) * HD ** (-0.5)
    first_row = lax.axis_index("ep") * row_count
    query_index = jnp.arange(span_len, dtype=jnp.int32)[:, None]
    key_index = jnp.arange(2 * span_len, dtype=jnp.int32)[None, :]
    distance = query_index + span_len - key_index
    key_place = (
        first_row
        + jnp.arange(blocks, dtype=jnp.int32)[:, None, None] * span_len
        + key_index[None]
        - span_len
    )
    allowed = (distance >= 0)[None] & (distance < span_len)[None] & (key_place >= 0)
    masked = jnp.where(allowed[:, None, None], scores, -1e30)
    sink_full = sink_logits.reshape(kv_local, group_size)[None, :, :, None]
    row_max = jnp.maximum(jnp.max(masked, axis=-1), sink_full)
    weights_exp = jnp.exp(masked - row_max[..., None])
    denominator = jnp.sum(weights_exp, axis=-1) + jnp.exp(sink_full - row_max)
    probs = (weights_exp / denominator[..., None]).astype(jnp.bfloat16)
    attended = jnp.einsum(
        "nhgqk,nkhd->nqhgd", probs, value_band, preferred_element_type=jnp.float32
    )
    attended = attended.astype(jnp.bfloat16).reshape(row_count, kv_local * group_size * HD)
    mixed = jnp.dot(
        lax.all_gather(attended, "tp", axis=1, tiled=True),
        out_weight,
        preferred_element_type=jnp.float32,
    )
    mixer_out = mixed.astype(jnp.bfloat16)
    tp_count = lax.axis_size("tp")
    tp_index = lax.axis_index("tp")
    exp_local = expert_gate.shape[0]
    expert_count = exp_local * lax.axis_size("ep")
    rows_dev = tokens_b.shape[0] // tp_count
    capacity = min(4 * rows_dev // expert_count, rows_dev // 4)
    own_routes = lax.dynamic_slice_in_dim(route_expert, tp_index * rows_dev, rows_dev, 0)
    own_normed = normalize(
        lax.dynamic_slice_in_dim(tokens_b, tp_index * rows_dev, rows_dev, 0), moe_gain
    )
    flat_routes, places = slot_positions(own_routes, 1, expert_count)
    buffer = fill_slots(own_normed, flat_routes, places, 1, expert_count, capacity, exp_local)
    delivered = lax.all_to_all(buffer, "ep", split_axis=0, concat_axis=0, tiled=True)
    arrived = lax.all_gather(delivered, "tp", axis=2, tiled=True)
    own_flat = flat_routes[0]
    own_places = places[0]
    gates = gate_weights(own_normed, own_routes, router_group, router_expert)
    gate_pre = jnp.einsum(
        "setcd,edf->setcf", arrived, expert_gate, preferred_element_type=jnp.float32
    )
    up_pre = jnp.einsum("setcd,edf->setcf", arrived, expert_up, preferred_element_type=jnp.float32)
    activated = (jax.nn.silu(gate_pre) * up_pre).astype(jnp.bfloat16)
    partial_value = jnp.einsum(
        "setcf,efd->setcd", activated, expert_down, preferred_element_type=jnp.float32
    )
    summed = summed_on_arrival(partial_value.astype(jnp.bfloat16), "tp", 2).astype(jnp.bfloat16)
    returned = lax.all_to_all(summed, "ep", split_axis=0, concat_axis=0, tiled=True)
    returned = returned.reshape(expert_count * capacity, returned.shape[-1])
    picked_rows = returned[own_flat * capacity + own_places].reshape(
        rows_dev, 2, returned.shape[-1]
    )
    moe_out = jnp.sum(gates[:, :, None] * picked_rows.astype(jnp.float32), axis=1).astype(
        jnp.bfloat16
    )
    return (mixer_out, moe_out)


def solution(mesh):
    in_specs = (
        P("ep", "tp"),
        P("ep", "tp"),
        P("ep", "tp"),
        P("tp"),
        P(None, "tp"),
        P("ep", None),
        P(),
        P(),
        P(),
        P("ep", None),
        P("ep", None, "tp"),
        P("ep", None, "tp"),
        P("ep", "tp", None),
    )
    out_specs = (P("ep", "tp"), P(("ep", "tp"), None))
    return jax.shard_map(
        per_device, mesh=mesh, in_specs=in_specs, out_specs=out_specs, check_vma=False
    )
```

profile of v0, /device:TPU:1, one launch (start us, length us, event | category | flops | bytes accessed | tf_op | source)
XLA Modules:
  0.0 391.8 jit_solution(18219090513013595579)
XLA Ops:
  7.2 0.8 broadcast_multiply_fusion
  8.1 0.1 copy.60
  8.2 0.1 eq.62
  8.3 0.1 fusion.41
  8.4 0.1 fusion.39
  8.6 0.2 fusion.38
  8.8 0.1 copy.59
  8.9 0.1 mul.115
  9.1 1.2 fusion.24
  10.3 1.3 fusion.26
  11.6 1.6 broadcast_in_dim.34
  13.2 2.3 reshape.388
  15.5 4.4 %scatter_custom_fusion = bf16[512,2048]{1,0:T(8,128)(2,1)} fusion(s32[256]{0:T(256)S(1)} %bitcast.167, bf16[256,2048]{1,0:T(8,128)(2,1)} %reshape.388, bf16[]{:T(256)} %constant.68.clone.1), kind=kCustom, calls=%fused_computation.35 | custom fusion | bytes 2097664 | tf_op jit(solution)/shard_map/scatter | solution.py:64
  19.9 4.1 %reshape.371 = bf16[64,2,1,4,2048]{4,3,1,0,2:T(4,128)(2,1)} reshape(bf16[512,2048]{1,0:T(8,128)(2,1)} %scatter_custom_fusion) | data formatting | bytes 4194304 | tf_op jit(solution)/shard_map/reshape | solution.py:65
  24.0 62.8 %all_to_all.15 = bf16[64,2,1,4,2048]{4,3,2,1,0:T(4,128)(2,1)S(1)} all-to-all(bf16[64,2,1,4,2048]{4,3,2,1,0:T(4,128)(2,1)} %bitcast.154), channel_id=1, replica_groups=mesh['ep'=64,'tp'=4] {'ep'}, dimensions={0} | all-to-all | bytes 4194304 | tf_op jit(solution)/shard_map/all_to_all | solution.py:144
  86.8 2.5 copy.64
  89.4 83.2 %all-gather.5.cloned.1.call-done = bf16[64,2,4,4,2048]{4,0,3,2,1:T(8,128)(2,1)} async-done(((bf16[64,2,1,4,2048]{4,0,3,2,1:T(8,128)(2,1)}), bf16[64,2,4,4,2048]{4,0,3,2,1:T(8,128)(2,1)}) %all-gather.5.cloned.1.call-update) | async-done | bytes 8388624 | tf_op jit(solution)/shard_map/all_gather | solution.py:145
  172.6 7.7 %fusion.3 = f32[2,64,4,4,256]{4,1,3,2,0:T(8,128)} fusion(bf16[64,2,4,4,2048]{4,0,3,2,1:T(8,128)(2,1)} %all-gather.5.cloned.1.call-done, bf16[2,2048,256]{2,1,0:T(8,128)(2,1)} %param.24), kind=kOutput, calls=%fused_computation.9 | convolution fusion | flops 2147483648 | bytes 12582912 | tf_op jit(solution)/shard_map/setcd,edf->setcf/dot_general | solution.py:152
  180.3 13.5 %convert_bitcast_fusion = bf16[4,64,2,1,4,2048]{5,1,4,0,2,3:T(8,128)(2,1)} fusion(bf16[2,256,2048]{2,1,0:T(8,128)(2,1)S(1)} %copy-done, f32[2,64,4,4,256]{4,1,3,2,0:T(8,128)} %fusion.3, bf16[64,2,4,4,2048]{4,0,3,2,1:T(8,128)(2,1)} %all-gather.5.cloned.1.call-done, bf16[2,2048,256]{2,1,0:T(8,128)(2,1)} %param.23), kind=kOutput, calls=%fused_computation.2 | convolution fusion | flops 4302307328 | bytes 23068672 | tf_op jit(solution)/shard_map/setcf,efd->setcd/dot_general | solution.py:154
  193.8 8.3 %copy.65 = bf16[4,64,2,1,4,2048]{5,1,4,2,3,0:T(8,128)(2,1)} copy(bf16[4,64,2,1,4,2048]{5,1,4,0,2,3:T(8,128)(2,1)} %convert_bitcast_fusion) | data formatting | bytes 16777216 | tf_op jit(solution)/shard_map/transpose | solution.py:20
  202.0 5.8 %all-to-all-start.1 = ((bf16[4,64,2,1,4,2048]{5,1,4,2,3,0:T(8,128)(2,1)}), bf16[4,64,2,1,4,2048]{5,1,4,2,3,0:T(8,128)(2,1)}, u32[]{:S(2)}, u32[]{:S(2)}) async-start(bf16[4,64,2,1,4,2048]{5,1,4,2,3,0:T(8,128)(2,1)} %copy.65), calls=%async_computation.1 | async-start | bytes 16777216 | tf_op jit(solution)/shard_map/all_to_all | solution.py:25
  207.9 4.1 %collective-permute-start = (bf16[2,128,64]{1,2,0:T(8,128)(2,1)S(1)}, bf16[2,128,64]{1,2,0:T(8,128)(2,1)S(1)}, u32[]{:S(2)}, u32[]{:S(2)}) collective-permute-start(bf16[2,128,64]{1,2,0:T(8,128)(2,1)S(1)} %pad_maximum_fusion.2), channel_id=1, source_target_pairs={{0,4},{4,8},{8,12},{12,16},{16,20},{20,24},{24,28},{28,32},{32,36}... | collective-permute-start | bytes 98312 | tf_op jit(solution)/shard_map/ppermute | solution.py:15
  212.0 0.1 add_compare_fusion
  212.1 0.3 broadcast_and_fusion
  212.5 0.4 reshape.397
  213.2 0.9 fusion.1
  214.2 1.1 fusion
  215.3 0.8 copy-done.2
  216.0 0.1 exponential_add_fusion
  216.1 84.8 %all-to-all-done.1 = bf16[4,64,2,1,4,2048]{5,1,4,2,3,0:T(8,128)(2,1)} async-done(((bf16[4,64,2,1,4,2048]{5,1,4,2,3,0:T(8,128)(2,1)}), bf16[4,64,2,1,4,2048]{5,1,4,2,3,0:T(8,128)(2,1)}, u32[]{:S(2)}, u32[]{:S(2)}) %all-to-all-start.1) | async-done | bytes 8388640 | tf_op jit(solution)/shard_map/all_to_all | solution.py:25
  300.9 5.6 %reduce_sum.93 = bf16[64,2,4,2048]{3,0,2,1:T(8,128)(2,1)S(1)} reduce(bf16[4,64,2,1,4,2048]{5,1,4,2,3,0:T(8,128)(2,1)} %all-to-all-done.1, bf16[]{:T(256)} %constant.68.clone.1), dimensions={0,3}, to_apply=%region_13.14 | reduce | flops 3145728 | bytes 10485762 | tf_op jit(solution)/shard_map/reduce_sum | solution.py:26
  306.5 2.9 copy.67
  309.4 11.9 %all-to-all-start.2 = ((bf16[64,2,1,4,2048]{4,3,1,2,0:T(4,128)(2,1)}), bf16[64,2,1,4,2048]{4,3,1,2,0:T(4,128)(2,1)}, u32[]{:S(2)}, u32[]{:S(2)}) async-start(bf16[64,2,1,4,2048]{4,3,1,2,0:T(4,128)(2,1)} %copy.67), calls=%async_computation.2 | async-start | bytes 4194304 | tf_op jit(solution)/shard_map/all_to_all | solution.py:158
  321.3 0.3 all-gather.3.cloned.1.call-start
  321.6 3.4 fusion.21
  325.0 0.3 copy.57
  325.4 0.9 copy.89
  326.3 0.3 fusion.55
  326.6 0.2 select_reduce_fusion
  326.9 0.3 fusion.54
  327.2 0.1 copy.58
  327.3 31.4 %all-gather.3.cloned.1.call-done = bf16[1024,1024]{0,1:T(8,128)(2,1)} async-done(((bf16[1024,256]{0,1:T(8,128)(2,1)}), bf16[1024,1024]{0,1:T(8,128)(2,1)}) %all-gather.3.cloned.1.call-update) | async-done | bytes 2097168 | tf_op jit(solution)/shard_map/all_gather | solution.py:127
  358.7 4.1 %convolution_convert_fusion = bf16[1024,512]{1,0:T(8,128)(2,1)} fusion(bf16[1024,1024]{0,1:T(8,128)(2,1)} %all-gather.3.cloned.1.call-done, bf16[1024,512]{1,0:T(8,128)(2,1)} %param.17), kind=kOutput, calls=%fused_computation.24 | convolution fusion | flops 1074266112 | bytes 4194304 | tf_op jit(solution)/shard_map/dot_general | solution.py:126
  362.8 8.2 %all-to-all-done.2 = bf16[64,2,1,4,2048]{4,3,1,2,0:T(4,128)(2,1)} async-done(((bf16[64,2,1,4,2048]{4,3,1,2,0:T(4,128)(2,1)}), bf16[64,2,1,4,2048]{4,3,1,2,0:T(4,128)(2,1)}, u32[]{:S(2)}, u32[]{:S(2)}) %all-to-all-start.2) | async-done | bytes 2097184 | tf_op jit(solution)/shard_map/all_to_all | solution.py:158
  371.0 2.5 reshape.373
  373.5 2.3 gather_fusion
  375.8 3.5 reshape.375
  379.4 5.6 %multiply_reduce_fusion = bf16[128,2048]{1,0:T(8,128)(2,1)} fusion(f32[128,2,2048]{2,1,0:T(2,128)} %reshape.375, f32[128,2]{1,0:T(8,128)S(1)} %copy.58), kind=kLoop, calls=%fused_computation.22 | loop fusion | flops 786432 | bytes 2622464 | tf_op jit(solution)/shard_map/reduce_sum | solution.py:163
  (53 shorter events, 0.7 us)
Async XLA Ops:
  7.2 173.1 %copy-start = (bf16[2,256,2048]{2,1,0:T(8,128)(2,1)S(1)}, bf16[2,256,2048]{2,1,0:T(8,128)(2,1)}, u32[]{:S(2)}) copy-start(bf16[2,256,2048]{2,1,0:T(8,128)(2,1)} %param.25) | copy-start | bytes 6291460
  7.2 165.4 %all-gather.5.cloned.1.call-start = ((), (), s32[]{:S(2)}) async-start(), calls=%async_computation.4 | async-start | bytes 10485760 | tf_op jit(solution)/shard_map/all_gather | solution.py:145
  202.0 5.8 %copy-start.3 = (bf16[1024,64]{0,1:T(8,128)(2,1)S(1)}, bf16[1024,64]{0,1:T(8,128)(2,1)}, u32[]{:S(2)}) copy-start(bf16[1024,64]{0,1:T(8,128)(2,1)} %param.14) | copy-start | bytes 393220
  202.0 5.8 %copy-start.4 = (bf16[1024,64]{0,1:T(8,128)(2,1)S(1)}, bf16[1024,64]{0,1:T(8,128)(2,1)}, u32[]{:S(2)}) copy-start(bf16[1024,64]{0,1:T(8,128)(2,1)} %param.15) | copy-start | bytes 393220
  202.0 10.5 %copy-start.5 = (bf16[1024,256]{1,0:T(8,128)(2,1)S(1)}, bf16[1024,256]{1,0:T(8,128)(2,1)}, u32[]{:S(2)}) copy-start(bf16[1024,256]{1,0:T(8,128)(2,1)} %param.13) | copy-start | bytes 1572868
  202.0 98.9 %all-to-all-start.1 = ((bf16[4,64,2,1,4,2048]{5,1,4,2,3,0:T(8,128)(2,1)}), bf16[4,64,2,1,4,2048]{5,1,4,2,3,0:T(8,128)(2,1)}, u32[]{:S(2)}, u32[]{:S(2)}) async-start(bf16[4,64,2,1,4,2048]{5,1,4,2,3,0:T(8,128)(2,1)} %copy.65), calls=%async_computation.1 | async-start | bytes 16777216 | tf_op jit(solution)/shard_map/all_to_all | solution.py:25
  207.9 5.1 %collective-permute-start = (bf16[2,128,64]{1,2,0:T(8,128)(2,1)S(1)}, bf16[2,128,64]{1,2,0:T(8,128)(2,1)S(1)}, u32[]{:S(2)}, u32[]{:S(2)}) collective-permute-start(bf16[2,128,64]{1,2,0:T(8,128)(2,1)S(1)} %pad_maximum_fusion.2), channel_id=1, source_target_pairs={{0,4},{4,8},{8,12},{12,16},{16,20},{20,24},{24,28},{28,32},{32,36}... | collective-permute-start | bytes 98312 | tf_op jit(solution)/shard_map/ppermute | solution.py:15
  213.2 0.9 copy-start.8
  214.1 1.9 copy-start.2
  309.4 61.5 %all-to-all-start.2 = ((bf16[64,2,1,4,2048]{4,3,1,2,0:T(4,128)(2,1)}), bf16[64,2,1,4,2048]{4,3,1,2,0:T(4,128)(2,1)}, u32[]{:S(2)}, u32[]{:S(2)}) async-start(bf16[64,2,1,4,2048]{4,3,1,2,0:T(4,128)(2,1)} %copy.67), calls=%async_computation.2 | async-start | bytes 4194304 | tf_op jit(solution)/shard_map/all_to_all | solution.py:158
  321.3 37.4 %all-gather.3.cloned.1.call-start = ((), (), s32[]{:S(2)}) async-start(), calls=%async_computation.3 | async-start | bytes 2621440 | tf_op jit(solution)/shard_map/all_gather | solution.py:127
  325.0 1.3 copy-start.6
  325.0 1.8 copy-start.7
  375.8 9.1 %copy-start.1 = (bf16[2,256,2048]{2,1,0:T(8,128)(2,1)S(1)}, bf16[2,256,2048]{2,1,0:T(8,128)(2,1)}, u32[]{:S(2)}) copy-start(bf16[2,256,2048]{2,1,0:T(8,128)(2,1)} %param.25) | copy-start | bytes 6291460
Sparse Core Ops, SparseCore 0:
  89.5 83.0 all-gather.4
  326.4 32.2 all-gather.2
where the time goes:
time: 393 us; the launch traced here: 392 us
  waiting for transfers between devices  208 us (53%)
  blocking collectives  62.8 us (16%)
  local copies, waits for them, and re-layouts  37.8 us (10%)
  matrix products  30.1 us (8%)
  starting transfers between devices  22.1 us (6%)
  other arithmetic  16.9 us (4%)
  between operations  14.4 us (4%)
    all_to_all x1, waiting for transfers between devices, summed_on_arrival(): parts = lax.all_to_all(in_blocks(array, dim, peers), axis, 0, 0, tiled=True)  84.8 us
    all_gather x1, waiting for transfers between devices, per_device(): arrived = lax.all_gather(delivered, 'tp', axis=2, tiled=True)  83.2 us
    all_to_all x1, blocking collectives, per_device(): lax.all_to_all(buffer, 'ep', split_axis=0, concat_axis=0, tiled=True)  62.8 us
    all_gather x1, waiting for transfers between devices, per_device(): lax.all_gather(attended, 'tp', axis=1, tiled=True)  31.4 us
    dot_general x1, matrix products, per_device(): jnp.einsum('setcf,efd->setcd', activated, expert_down, preferred_element_...  13.5 us
    all_to_all x1, starting transfers between devices, per_device(): lax.all_to_all(summed, 'ep', split_axis=0, concat_axis=0, tiled=True)  11.9 us
    transpose x1, local copies, waits for them, and re-layouts, in_blocks(): return jnp.moveaxis(array.reshape(*before, peers, -1, *after), dim, 0)  8.26 us
    all_to_all x1, waiting for transfers between devices, per_device(): lax.all_to_all(summed, 'ep', split_axis=0, concat_axis=0, tiled=True)  8.16 us
  transfers between devices with their start and end apart: 5, of which 4 were waited for; matrix products, arithmetic and copies ran while one was open for 3% of the time, Pallas kernels for 0%

commit v1 on v0

v1 whole, which is shorter than its diff:
```python
import functools

import jax
import jax.numpy as jnp
from jax import lax
from jax.experimental import pallas as pl
from jax.experimental.pallas import tpu as pltpu
from jax.sharding import PartitionSpec as P

HEADS = 16
KV = 4
HD = 64
WINDOW = 128
CAP = 4
GROUPS = 4
NTP = 4
PLANE = 8
MESH = pl.DeviceIdType.MESH
F32 = jnp.float32
BF16 = jnp.bfloat16


def shifted(value, axis, steps):
    count = lax.axis_size(axis)
    leading, last = (max(0, -steps), min(count, count - steps))
    return lax.ppermute(value, axis, [(source, source + steps) for source in range(leading, last)])


def hop_of(i, nz):
    if i == 0:
        return 0
    return (nz - i) // 2 if i % 2 == 0 else (i + nz - 1) // 2


def position_of(d, nz):
    return jnp.where(d == 0, 0, jnp.where(d < nz // 2, nz - 2 * d, 2 * d - nz + 1))


def slot_rows(expert, block, place, z, yc, nz, nyc):
    rank = expert >> 1
    d = lax.rem(lax.div(rank, nyc) - z + nz, nz)
    j = lax.rem(lax.rem(rank, nyc) - yc + nyc, nyc)
    return ((position_of(d, nz) * nyc + j) * 2 + (expert & 1)) * (NTP * CAP) + block * CAP + place


def prep_kernel(nz, nyc, tok, gain, routes_t, routes, r_group, r_expert, slots, gates, rows_out, normed):
    x = lax.axis_index("tp")
    e = lax.axis_index("ep")
    z, yc = lax.div(e, nyc), lax.rem(e, nyc)
    tokens, width = tok.shape
    block_rows = tokens // NTP
    experts = r_expert.shape[1]
    fq = width // NTP
    step = tokens // 8

    def norm_rows(i, carry):
        rows = pl.ds(pl.multiple_of(i * step, step), step)
        v = tok[rows, :].astype(F32)
        ms = jnp.mean(v * v, axis=-1, keepdims=True)
        normed[rows, :] = (v * lax.rsqrt(ms + 1e-06) * gain[...]).astype(BF16)
        return carry

    lax.fori_loop(0, 8, norm_rows, 0)

    def iota(shape, dim):
        return lax.broadcasted_iota(jnp.int32, shape, dim)

    first, second = (iota((tokens, tokens), 0), iota((tokens, tokens), 1))
    same = lax.div(first, block_rows) == lax.div(second, block_rows)
    e0, e1 = routes_t[0:1, :], routes_t[1:2, :]
    ids = iota((experts, tokens), 0)
    hit0, hit1 = ids == e0, ids == e1
    before = jnp.where(same & (first < second), 1.0, 0.0).astype(BF16)
    both = jnp.where(hit0 | hit1, 1.0, 0.0).astype(BF16)
    count = jnp.dot(both, before, preferred_element_type=F32)
    place0 = jnp.sum(jnp.where(hit0, count, 0.0), axis=0, keepdims=True).astype(jnp.int32)
    place1 = jnp.sum(jnp.where(hit1, count, 0.0), axis=0, keepdims=True).astype(jnp.int32)
    block = lax.div(iota((1, tokens), 1), block_rows)
    t0 = slot_rows(e0, block, place0, z, yc, nz, nyc)
    t1 = slot_rows(e1, block, place1, z, yc, nz, nyc)
    part = nyc * 2 * NTP * CAP
    mine = normed[:, pl.ds(pl.multiple_of(x * fq, fq), fq)]

    def fill(i, carry):
        ids = iota((part, tokens), 0) + i * part
        pick = jnp.where((ids == t0) | (ids == t1), 1.0, 0.0).astype(BF16)
        got = jnp.dot(pick, mine, preferred_element_type=F32).astype(BF16)
        slots[i] = got.reshape(nyc, 2, NTP * CAP, fq)
        return carry

    lax.fori_loop(0, nz, fill, 0)
    c0, c1 = routes[:, 0:1], routes[:, 1:2]
    ids = iota((tokens, experts), 1)
    hit0, hit1 = ids == c0, ids == c1
    after = jnp.where(same & (second < first), 1.0, 0.0).astype(BF16)
    both = jnp.where(hit0 | hit1, 1.0, 0.0).astype(BF16)
    count = jnp.dot(after, both, preferred_element_type=F32)
    place0 = jnp.sum(jnp.where(hit0, count, 0.0), axis=1, keepdims=True).astype(jnp.int32)
    place1 = jnp.sum(jnp.where(hit1, count, 0.0), axis=1, keepdims=True).astype(jnp.int32)
    block = lax.div(iota((tokens, 1), 0), block_rows)
    rows_out[:, 0:1] = slot_rows(c0, block, place0, z, yc, nz, nyc)
    rows_out[:, 1:2] = slot_rows(c1, block, place1, z, yc, nz, nyc)
    by_expert = jnp.dot(normed[...], r_expert[...], preferred_element_type=F32)
    by_group = jnp.dot(normed[...], r_group[...], preferred_element_type=F32)
    groups = r_group.shape[1]
    group_max = jnp.max(by_group, axis=1, keepdims=True)
    group_exp = jnp.exp(by_group - group_max)
    chosen = iota((tokens, groups), 1) == lax.div(c0, experts // groups)
    share = jnp.sum(jnp.where(chosen, group_exp, 0.0), axis=1, keepdims=True) / jnp.sum(
        group_exp, axis=1, keepdims=True
    )
    l0 = jnp.sum(jnp.where(hit0, by_expert, 0.0), axis=1, keepdims=True)
    l1 = jnp.sum(jnp.where(hit1, by_expert, 0.0), axis=1, keepdims=True)
    top = jnp.maximum(l0, l1)
    x0, x1 = jnp.exp(l0 - top), jnp.exp(l1 - top)
    gates[:, 0:1] = share * (x0 / (x0 + x1))
    gates[:, 1:2] = share * (x1 / (x0 + x1))


def moe_kernel(
    nz, nyc, s_hbm, wg_hbm, wu_hbm, wd_hbm, att_hbm, ow_hbm, gates, rows_in, mix, moe,
    relay, arr, wg, wu, wq, act, out, back, ret, att, ow, fin_out, fin,
    zs, zr, ys, yr, xs, xr, fs, fr, acs, acr, afs, afr, ws, wr,
    rzs, rzr, rys, ryr, ts, tr, tfs, tfr, es, er, loc,
):
    x = lax.axis_index("tp")
    e = lax.axis_index("ep")
    z, yc = lax.div(e, nyc), lax.rem(e, nyc)
    fq = arr.shape[-1]
    hq = wg.shape[-1]
    hops = [hop_of(i, nz) for i in range(nz)]
    half = nyc // 2
    pairs = nz // 2

    def zdev(d):
        return (lax.rem(z + (d + nz), nz) * nyc + yc, x)

    def ydev(j):
        return (z * nyc + lax.rem(yc + (j + nyc), nyc), x)

    def xdev(q):
        return (e, lax.rem(x + q, NTP))

    def column(q):
        return lax.rem(x + q, NTP)

    def send(src, dst, s_sem, r_sem, dev):
        copy = pltpu.make_async_remote_copy(
            src_ref=src, dst_ref=dst, send_sem=s_sem, recv_sem=r_sem,
            device_id=dev, device_id_type=MESH,
        )
        copy.start()

    def drain(ref, sem):
        pltpu.make_async_copy(ref, ref, sem).wait()

    barrier = pltpu.get_barrier_semaphore()
    peers = [zdev(d) for d in range(1, nz)] + [ydev(j) for j in range(1, nyc)]
    peers += [xdev(q) for q in range(1, NTP)]
    for peer in peers:
        pl.semaphore_signal(barrier, inc=1, device_id=peer, device_id_type=MESH)
    local = [
        pltpu.make_async_copy(s_hbm.at[0, 0], arr.at[0, 0, 0], loc.at[0]),
        pltpu.make_async_copy(wg_hbm, wg, loc.at[1]),
        pltpu.make_async_copy(wu_hbm, wu, loc.at[2]),
        pltpu.make_async_copy(
            wd_hbm.at[:, :, pl.ds(pl.multiple_of(x * fq, fq), fq)], wq.at[0], loc.at[3]
        ),
        pltpu.make_async_copy(att_hbm, att.at[0], loc.at[4]),
        pltpu.make_async_copy(ow_hbm, ow, loc.at[5]),
    ]
    for copy in local:
        copy.start()
    pl.semaphore_wait(barrier, len(peers))

    for i in range(1, nz):
        send(s_hbm.at[i, 0], arr.at[0, i, 0], zs.at[i, 0], zr.at[i, 0], zdev(hops[i]))
        send(
            s_hbm.at[i, pl.ds(1, nyc - 1)], relay.at[i, pl.ds(1, nyc - 1)],
            zs.at[i, 1], zr.at[i, 1], zdev(hops[i]),
        )
    for j in range(1, nyc):
        send(s_hbm.at[0, j], arr.at[0, 0, j], ys.at[0], yr.at[0], ydev(j))
    for q in range(1, NTP):
        cols = pl.ds(pl.multiple_of(column(q) * fq, fq), fq)
        send(wd_hbm.at[:, :, cols], wq.at[q], ws.at[q], wr.at[q], xdev(q))

    def plane_out(i):
        if i == 0:
            return
        drain(relay.at[i, pl.ds(1, nyc - 1)], zr.at[i, 1])
        for j in range(1, nyc):
            send(relay.at[i, j], arr.at[0, i, j], ys.at[i], yr.at[i], ydev(j))

    def ring_own(i):
        if i == 0:
            local[0].wait()
        else:
            drain(arr.at[0, i, 0], zr.at[i, 0])
        drain(arr.at[0, i, pl.ds(1, nyc - 1)], yr.at[i])
        send(arr.at[0, i], arr.at[1, i], xs.at[i, 0], xr.at[i, 0], xdev(1))
        send(arr.at[0, i], arr.at[3, i], xs.at[i, 1], xr.at[i, 1], xdev(3))

    def ring_on(i):
        low, high = pl.ds(0, half), pl.ds(half, half)
        drain(arr.at[1, i], xr.at[i, 0])
        send(arr.at[1, i, low], arr.at[2, i, low], fs.at[i, 0], fr.at[i, 0], xdev(1))
        drain(arr.at[3, i], xr.at[i, 1])
        send(arr.at[3, i, high], arr.at[2, i, high], fs.at[i, 1], fr.at[i, 1], xdev(3))

    def ring_in(i):
        drain(arr.at[2, i, pl.ds(0, half)], fr.at[i, 0])
        drain(arr.at[2, i, pl.ds(half, half)], fr.at[i, 1])

    rows2 = 2 * nyc * NTP * CAP

    def hidden(p):
        if p == 0:
            local[1].wait()
            local[2].wait()

        def one(k, carry):
            gate = jnp.zeros((rows2, hq), F32)
            up = jnp.zeros((rows2, hq), F32)
            for q in range(NTP):
                depth = pl.ds(pl.multiple_of(column(NTP - q) * fq, fq), fq)
                rows = arr[q, pl.ds(2 * p, 2), :, k].reshape(rows2, fq)
                gate += jnp.dot(rows, wg[k, depth, :], preferred_element_type=F32)
                up += jnp.dot(rows, wu[k, depth, :], preferred_element_type=F32)
            value = (gate / (1.0 + jnp.exp(-gate)) * up).astype(BF16)
            act[0, p, k] = value
            return carry

        lax.fori_loop(0, 2, one, 0)
        send(act.at[0, p], act.at[1, p], acs.at[p, 0], acr.at[p, 0], xdev(1))
        send(act.at[0, p], act.at[3, p], acs.at[p, 1], acr.at[p, 1], xdev(3))

    def act_on(p):
        drain(act.at[1, p], acr.at[p, 0])
        send(act.at[1, p, 0], act.at[2, p, 0], afs.at[p, 0], afr.at[p, 0], xdev(1))
        drain(act.at[3, p], acr.at[p, 1])
        send(act.at[3, p, 1], act.at[2, p, 1], afs.at[p, 1], afr.at[p, 1], xdev(3))

    def down(p):
        if p == 0:
            local[3].wait()
            for q in range(1, NTP):
                drain(wq.at[q], wr.at[q])
        drain(act.at[2, p, 0], afr.at[p, 0])
        drain(act.at[2, p, 1], afr.at[p, 1])

        def one(k, carry):
            total = jnp.zeros((rows2, fq), F32)
            for q in range(NTP):
                total += jnp.dot(act[q, p, k], wq[q, k], preferred_element_type=F32)
            out[pl.ds(2 * p, 2), :, k] = total.astype(BF16).reshape(2, nyc, NTP * CAP, fq)
            return carry

        lax.fori_loop(0, 2, one, 0)
        for i in (2 * p, 2 * p + 1):
            if i == 0:
                ret[0, 0] = out[0, 0]
                for j in range(1, nyc):
                    send(out.at[0, j], ret.at[0, j], rys.at[0], ryr.at[0], ydev(-j))
                continue
            rest = pl.ds(1, nyc - 1)
            send(out.at[i, rest], back.at[i, rest], rzs.at[i, 1], rzr.at[i, 1], zdev(-hops[i]))
            send(out.at[i, 0], ret.at[i, 0], rzs.at[i, 0], rzr.at[i, 0], zdev(-hops[i]))

    def plane_back(i):
        if i == 0:
            return
        drain(back.at[i, pl.ds(1, nyc - 1)], rzr.at[i, 1])
        for j in range(1, nyc):
            send(back.at[i, j], ret.at[i, j], rys.at[i], ryr.at[i], ydev(-j))

    for n in range(nz + 2):
        if n < nz:
            plane_out(n)
        if 0 <= n - 1 < nz:
            ring_own(n - 1)
        if 0 <= n - 2 < nz:
            ring_on(n - 2)
        m = n - 3
        if m >= 0:
            ring_in(m)
            if m % 2 == 1:
                hidden(m // 2)
                if m >= 3:
                    down(m // 2 - 1)
            elif m >= 2:
                act_on(m // 2 - 1)
    ring_in(nz - 1)
    hidden(pairs - 1)
    if pairs > 1:
        down(pairs - 2)
    act_on(pairs - 1)
    rows = att.shape[1]
    top, bottom = pl.ds(0, rows // 2), pl.ds(rows // 2, rows // 2)
    send(att_hbm, att.at[1], ts.at[0], tr.at[0], xdev(1))
    send(att_hbm, att.at[3], ts.at[1], tr.at[1], xdev(3))
    for i in range(nz - 2):
        plane_back(i)
    down(pairs - 1)
    drain(att.at[1], tr.at[0])
    send(att.at[1, top], att.at[2, top], tfs.at[0], tfr.at[0], xdev(1))
    drain(att.at[3], tr.at[1])
    send(att.at[3, bottom], att.at[2, bottom], tfs.at[1], tfr.at[1], xdev(3))
    for i in range(nz - 2, nz):
        plane_back(i)
    local[4].wait()
    local[5].wait()
    drain(att.at[2, top], tfr.at[0])
    drain(att.at[2, bottom], tfr.at[1])
    chunk = rows // 4
    hw = att.shape[2]

    def project(c, carry):
        where = pl.ds(pl.multiple_of(c * chunk, chunk), chunk)
        total = jnp.zeros((chunk, ow.shape[1]), F32)
        for q in range(NTP):
            depth = pl.ds(pl.multiple_of(column(NTP - q) * hw, hw), hw)
            total += jnp.dot(att[q, where, :], ow[depth, :], preferred_element_type=F32)
        mix[where, :] = total.astype(BF16)
        return carry

    lax.fori_loop(0, 4, project, 0)

    for i in range(nz):
        if i > 0:
            drain(ret.at[i, 0], rzr.at[i, 0])
        drain(ret.at[i, pl.ds(1, nyc - 1)], ryr.at[i])

    slots = nz * nyc * 2 * NTP * CAP
    block_rows = gates.shape[0] // NTP

    def combined(t):
        where = pl.ds(pl.multiple_of(t * block_rows, block_rows), block_rows)
        ids = lax.broadcasted_iota(jnp.int32, (block_rows, slots), 1)
        at = rows_in[where, :]
        pick = jnp.concatenate(
            [jnp.where(ids == at[:, k : k + 1], 1.0, 0.0).astype(BF16) for k in range(2)], axis=0
        )
        got = jnp.dot(pick, ret[...].reshape(slots, fq), preferred_element_type=F32)
        g = gates[where, :]
        return (g[:, 0:1] * got[:block_rows] + g[:, 1:2] * got[block_rows:]).astype(BF16)

    for q in range(1, NTP):
        fin_out[q] = combined(column(q))
        send(fin_out.at[q], fin.at[q], es.at[q], er.at[q], xdev(q))
    moe[:, pl.ds(pl.multiple_of(x * fq, fq), fq)] = combined(x)
    for q in range(1, NTP):
        drain(fin.at[q], er.at[q])
        moe[:, pl.ds(pl.multiple_of(column(NTP - q) * fq, fq), fq)] = fin[q]

    rest = pl.ds(1, nyc - 1)
    for i in range(nz):
        if i > 0:
            drain(relay.at[i, 0], zs.at[i, 0])
            drain(relay.at[i, rest], zs.at[i, 1])
            drain(out.at[i, 0], rzs.at[i, 0])
            drain(out.at[i, rest], rzs.at[i, 1])
        drain(arr.at[0, i, rest], ys.at[i])
        drain(ret.at[i, rest], rys.at[i])
        for way in range(2):
            drain(arr.at[0, i], xs.at[i, way])
            drain(arr.at[0, i, pl.ds(0, half)], fs.at[i, way])
    for p in range(pairs):
        for way in range(2):
            drain(act.at[0, p], acs.at[p, way])
            drain(act.at[0, p, 0], afs.at[p, way])
    for way in range(2):
        drain(att.at[0], ts.at[way])
        drain(att.at[0, top], tfs.at[way])
    for q in range(1, NTP):
        drain(wq.at[q], ws.at[q])
        drain(fin_out.at[q], es.at[q])


def attention(q_heads, k_heads, v_heads, sink_logits):
    span_len = WINDOW
    row_count = q_heads.shape[0]
    kv_local = k_heads.shape[1] // HD
    group_size = HEADS // KV
    blocks = row_count // span_len
    stacked = jnp.stack([k_heads[row_count - span_len :], v_heads[row_count - span_len :]])
    earlier = shifted(stacked, "ep", 1)

    def make_band(own_rows, prev_rows):
        extended = jnp.concatenate([prev_rows, own_rows], axis=0).reshape(
            blocks + 1, span_len, kv_local, HD
        )
        return jnp.concatenate([extended[:-1], extended[1:]], axis=1)

    key_band = make_band(k_heads, earlier[0])
    value_band = make_band(v_heads, earlier[1])
    query_blocks = q_heads.reshape(blocks, span_len, kv_local, group_size, HD)
    scores = jnp.einsum(
        "nqhgd,nkhd->nhgqk", query_blocks, key_band, preferred_element_type=jnp.float32
    ) * HD ** (-0.5)
    first_row = lax.axis_index("ep") * row_count
    query_index = jnp.arange(span_len, dtype=jnp.int32)[:, None]
    key_index = jnp.arange(2 * span_len, dtype=jnp.int32)[None, :]
    distance = query_index + span_len - key_index
    key_place = (
        first_row
        + jnp.arange(blocks, dtype=jnp.int32)[:, None, None] * span_len
        + key_index[None]
        - span_len
    )
    allowed = (distance >= 0)[None] & (distance < span_len)[None] & (key_place >= 0)
    masked = jnp.where(allowed[:, None, None], scores, -1e30)
    sink_full = sink_logits.reshape(kv_local, group_size)[None, :, :, None]
    row_max = jnp.maximum(jnp.max(masked, axis=-1), sink_full)
    weights_exp = jnp.exp(masked - row_max[..., None])
    denominator = jnp.sum(weights_exp, axis=-1) + jnp.exp(sink_full - row_max)
    probs = (weights_exp / denominator[..., None]).astype(jnp.bfloat16)
    attended = jnp.einsum(
        "nhgqk,nkhd->nqhgd", probs, value_band, preferred_element_type=jnp.float32
    )
    return attended.astype(jnp.bfloat16).reshape(row_count, kv_local * group_size * HD)


def per_device(
    q_heads,
    k_heads,
    v_heads,
    sink_logits,
    out_weight,
    tokens_b,
    moe_gain,
    router_group,
    router_expert,
    route_expert,
    expert_gate,
    expert_up,
    expert_down,
):
    nyc = min(PLANE, lax.axis_size("ep"))
    nz = lax.axis_size("ep") // nyc
    tokens, width = tokens_b.shape
    fq = width // NTP
    hq = expert_gate.shape[2]
    sixteen = NTP * CAP
    attended = attention(q_heads, k_heads, v_heads, sink_logits)
    vmem = pl.BlockSpec(memory_space=pltpu.VMEM)
    anywhere = pl.BlockSpec(memory_space=pl.ANY)
    slots, gates, rows = pl.pallas_call(
        functools.partial(prep_kernel, nz, nyc),
        out_shape=(
            jax.ShapeDtypeStruct((nz, nyc, 2, sixteen, fq), BF16),
            jax.ShapeDtypeStruct((tokens, 2), F32),
            jax.ShapeDtypeStruct((tokens, 2), jnp.int32),
        ),
        in_specs=[vmem] * 6,
        out_specs=(vmem, vmem, vmem),
        scratch_shapes=[pltpu.VMEM((tokens, width), BF16)],
        compiler_params=pltpu.CompilerParams(vmem_limit_bytes=48 * 2**20),
        name="prep",
    )(
        tokens_b,
        moe_gain.reshape(1, width),
        route_expert.T,
        route_expert,
        router_group,
        router_expert,
    )
    dma = pltpu.SemaphoreType.DMA
    pairs = nz // 2
    rows2 = 2 * nyc * sixteen
    slot = (nz, nyc, 2, sixteen, fq)
    mixer_out, moe_out = pl.pallas_call(
        functools.partial(moe_kernel, nz, nyc),
        out_shape=(
            jax.ShapeDtypeStruct((attended.shape[0], out_weight.shape[1]), BF16),
            jax.ShapeDtypeStruct((tokens // NTP, width), BF16),
        ),
        in_specs=[anywhere] * 6 + [vmem] * 2,
        out_specs=(vmem, vmem),
        scratch_shapes=[
            pltpu.VMEM(slot, BF16),
            pltpu.VMEM((NTP, *slot), BF16),
            pltpu.VMEM(expert_gate.shape, BF16),
            pltpu.VMEM(expert_up.shape, BF16),
            pltpu.VMEM((NTP, 2, hq, fq), BF16),
            pltpu.VMEM((NTP, pairs, 2, rows2, hq), BF16),
            pltpu.VMEM(slot, BF16),
            pltpu.VMEM(slot, BF16),
            pltpu.VMEM(slot, BF16),
            pltpu.VMEM((NTP, *attended.shape), BF16),
            pltpu.VMEM(out_weight.shape, BF16),
            pltpu.VMEM((NTP, tokens // NTP, fq), BF16),
            pltpu.VMEM((NTP, tokens // NTP, fq), BF16),
            dma((nz, 2)), dma((nz, 2)), dma((nz,)), dma((nz,)),
            dma((nz, 2)), dma((nz, 2)), dma((nz, 2)), dma((nz, 2)),
            dma((pairs, 2)), dma((pairs, 2)), dma((pairs, 2)), dma((pairs, 2)),
            dma((NTP,)), dma((NTP,)),
            dma((nz, 2)), dma((nz, 2)), dma((nz,)), dma((nz,)),
            dma((2,)), dma((2,)), dma((2,)), dma((2,)),
            dma((NTP,)), dma((NTP,)), dma((6,)),
        ],
        compiler_params=pltpu.CompilerParams(
            collective_id=0, has_side_effects=True, vmem_limit_bytes=60 * 2**20
        ),
        name="experts",
    )(slots, expert_gate, expert_up, expert_down, attended, out_weight, gates, rows)
    return (mixer_out, moe_out)


def solution(mesh):
    in_specs = (
        P("ep", "tp"),
        P("ep", "tp"),
        P("ep", "tp"),
        P("tp"),
        P(None, "tp"),
        P("ep", None),
        P(),
        P(),
        P(),
        P("ep", None),
        P("ep", None, "tp"),
        P("ep", None, "tp"),
        P("ep", "tp", None),
    )
    out_specs = (P("ep", "tp"), P(("ep", "tp"), None))
    return jax.shard_map(
        per_device, mesh=mesh, in_specs=in_specs, out_specs=out_specs, check_vma=False
    )
```

time: 393 us -> 205 us (0.52)
  waiting for transfers between devices: 208 us -> 0.01 us
  Pallas kernels: 0 us -> 177 us
  blocking collectives: 62.8 us -> 0 us
  matrix products: 30.1 us -> 2.1 us
  local copies, waits for them, and re-layouts: 37.8 us -> 17.3 us
  starting transfers between devices: 22.1 us -> 4.57 us
  other arithmetic: 16.9 us -> 2.98 us
  between operations: 14.4 us -> 0.94 us
    pallas_call x0 -> x2, Pallas kernels: none -> 177 us  [the longest x1 171 us: per_device(): pl.pallas_call(functools.partial(moe_kernel, nz, nyc), out_shape=(jax.Sha...]
    all_gather x2 -> x0, waiting for transfers between devices: 115 us -> none  [the longest x1 83.2 us: per_device(): arrived = lax.all_gather(delivered, 'tp', axis=2, tiled=True)]
    all_to_all x2 -> x0, waiting for transfers between devices: 93 us -> none  [the longest x1 84.8 us: summed_on_arrival(): parts = lax.all_to_all(in_blocks(array, dim, peers), axis, 0, 0, tiled=True)]
    all_to_all x1 -> x0, blocking collectives: 62.8 us -> none  [per_device(): lax.all_to_all(buffer, 'ep', split_axis=0, concat_axis=0, tiled=True)]
    dot_general x7 -> x2, matrix products: 30.1 us -> 2.1 us  [the longest x1 1.2 us: attention(): jnp.einsum('nhgqk,nkhd->nqhgd', probs, value_band, preferred_element_type...]
    all_to_all x2 -> x0, starting transfers between devices: 17.7 us -> none  [the longest x1 11.9 us: per_device(): lax.all_to_all(summed, 'ep', split_axis=0, concat_axis=0, tiled=True)]
    reduce_sum x9 -> x1, other arithmetic: 13.9 us -> 1.02 us  [attention(): denominator = jnp.sum(weights_exp, axis=-1) + jnp.exp(sink_full - row_max)]
    transpose x1 -> x0, local copies, waits for them, and re-layouts: 8.26 us -> none  [in_blocks(): return jnp.moveaxis(array.reshape(*before, peers, -1, *after), dim, 0)]
  transfers between devices with their start and end apart: 5 -> 1, of which waited for: 4 -> 0; matrix products, arithmetic and copies ran while one was open for 3% -> 4% of each run, Pallas kernels for 0% -> 3%
where the time goes in v1:
time: 205 us
  Pallas kernels  177 us (86%)
  local copies, waits for them, and re-layouts  17.3 us (8%)
  starting transfers between devices  4.57 us (2%)
  other arithmetic  2.98 us (1%)
  matrix products  2.1 us (1%)
    pallas_call x1, Pallas kernels, per_device(): pl.pallas_call(functools.partial(moe_kernel, nz, nyc), out_shape=(jax.Sha...  171 us
    unnamed x36, local copies, waits for them, and re-layouts  9.32 us
    pallas_call x1, Pallas kernels, per_device(): pl.pallas_call(functools.partial(prep_kernel, nz, nyc), out_shape=(jax.Sh...  6.22 us
    ppermute x1, starting transfers between devices, shifted(): lax.ppermute(value, axis, [(source, source + steps) for source in range(l...  4.57 us
  transfers between devices with their start and end apart: 1, of which 0 were waited for; matrix products, arithmetic and copies ran while one was open for 4% of the time, Pallas kernels for 3%

profile of v1, /device:TPU:1, one launch (start us, length us, event | category | flops | bytes accessed | tf_op | source)
XLA Modules:
  0.0 204.9 jit_solution(11568475269637839371)
XLA Ops:
  0.6 0.0 copy-start.9
  0.6 0.0 copy-start.1
  0.7 0.0 copy-start.2
  0.7 0.9 slice_bitcast_fusion.2
  1.6 0.6 pad_maximum_fusion.2
  2.2 4.6 %collective-permute-start = (bf16[2,128,64]{1,2,0:T(8,128)(2,1)}, bf16[2,128,64]{1,2,0:T(8,128)(2,1)}, u32[]{:S(2)}, u32[]{:S(2)}) collective-permute-start(bf16[2,128,64]{1,2,0:T(8,128)(2,1)} %pad_maximum_fusion.2), channel_id=1, source_target_pairs={{0,4},{4,8},{8,12},{12,16},{16,20},{20,24},{24,28},{28,32},{32,36}... | collective-permute-start | bytes 98312 | tf_op jit(solution)/shard_map/ppermute | solution.py:26
  6.8 0.1 add_compare_fusion
  6.9 1.0 broadcast_and_fusion
  7.9 2.8 %reshape.135 = bf16[8,128,4,64]{3,2,1,0:T(4,128)(2,1)} reshape(bf16[1024,256]{1,0:T(8,128)(2,1)} %param.13) | data formatting | bytes 1048576 | tf_op jit(solution)/shard_map/reshape.15
  10.7 0.9 copy.41
  11.6 0.7 copy.25
  12.3 0.9 copy.39
  13.2 0.7 copy.23
  13.9 1.0 copy.21.r_group
  14.9 0.8 copy.20.routes
  15.8 0.0 copy-done.1
  15.8 0.0 copy-done.2
  15.8 0.0 copy-start.5
  15.8 0.7 copy-done.5
  16.5 0.7 copy-done.6
  17.2 6.2 %prep.1 = (bf16[8,8,2,16,512]{4,3,2,1,0:T(8,128)(2,1)S(1)}, f32[512,2]{1,0:T(8,128)S(1)}, s32[512,2]{1,0:T(8,128)S(1)}) custom-call(bf16[512,2048]{1,0:T(8,128)(2,1)S(1)} %copy-done.1, f32[1,2048]{1,0:T(1,128)S(1)} %bitcast.77, s32[2,512]{1,0:T(2,128)S(1)} %bitcast.76, s32[512,2]{1,0:T(8,128)S(1)} %copy.20.routes, bf16[2048,4]{1,0:T(8,128)(2,1)S(1)} %copy.21.r_group, ...), custom_call_target="tpu_custom_call" | custom-call | tf_op jit(solution)/shard_map/prep/pallas_call | solution.py:448
  23.4 0.0 copy-start
  23.4 0.0 copy-start.3
  23.4 0.0 copy-start.4
  23.4 0.0 copy-start.13
  23.5 0.0 collective-permute-done
  23.5 0.8 slice_bitcast_fusion.1
  24.3 0.0 copy-done.9
  24.4 0.0 copy-done.7
  24.4 0.0 copy-done.8
  24.4 0.0 copy-done.12
  24.4 0.0 copy-start.10
  24.4 0.0 copy-start.11
  24.4 0.9 fusion.1
  25.3 0.0 copy-done.13
  25.3 0.1 broadcast_maximum_fusion
  25.4 1.0 fusion
  26.4 0.0 copy-done
  26.4 0.0 copy-done.3
  26.5 0.0 copy-done.4
  26.5 0.1 exponential_add_fusion
  26.6 0.0 copy-done.10
  26.7 1.2 fusion.8
  27.9 0.7 copy.36
  28.5 1.5 reshape.136.att_hbm
  30.0 170.7 %experts.1 = (bf16[1024,512]{1,0:T(8,128)(2,1)}, bf16[128,2048]{1,0:T(8,128)(2,1)}) custom-call(bf16[8,8,2,16,512]{4,3,2,1,0:T(8,128)(2,1)} %copy-done, bf16[2,2048,256]{2,1,0:T(8,128)(2,1)} %wg_hbm.1, bf16[2,2048,256]{2,1,0:T(8,128)(2,1)} %wu_hbm.1, bf16[2,256,2048]{2,1,0:T(8,128)(2,1)} %wd_hbm.1, bf16[1024,256]{1,0:T(8,128)(2,1)} %reshape.136.att_hbm, ...), custom_call_target="tpu_custom_call" | custom-call | tf_op jit(solution)/shard_map/experts/pallas_call | solution.py:472
  200.8 2.3 %copy.48 = bf16[1024,512]{1,0:T(8,128)(2,1)} copy(bf16[1024,512]{1,0:T(8,128)(2,1)} %get-tuple-element.16) | data formatting | bytes 2097152
  203.0 1.9 copy.49
  (14 shorter events, 0.2 us)
Async XLA Ops:
  0.6 23.7 %copy-start.9 = (bf16[1024,64]{0,1:T(8,128)(2,1)S(1)}, bf16[1024,64]{0,1:T(8,128)(2,1)}, u32[]{:S(2)}) copy-start(bf16[1024,64]{0,1:T(8,128)(2,1)} %param.14) | copy-start | bytes 393220
  0.6 15.1 %copy-start.1 = (bf16[512,2048]{1,0:T(8,128)(2,1)S(1)}, bf16[512,2048]{1,0:T(8,128)(2,1)}, u32[]{:S(2)}) copy-start(bf16[512,2048]{1,0:T(8,128)(2,1)} %tok.1) | copy-start | bytes 6291460
  0.7 15.1 %copy-start.2 = (bf16[2048,128]{1,0:T(8,128)(2,1)S(1)}, bf16[2048,128]{1,0:T(8,128)(2,1)}, u32[]{:S(2)}) copy-start(bf16[2048,128]{1,0:T(8,128)(2,1)} %r_expert.1) | copy-start | bytes 1572868
  2.2 21.3 %collective-permute-start = (bf16[2,128,64]{1,2,0:T(8,128)(2,1)}, bf16[2,128,64]{1,2,0:T(8,128)(2,1)}, u32[]{:S(2)}, u32[]{:S(2)}) collective-permute-start(bf16[2,128,64]{1,2,0:T(8,128)(2,1)} %pad_maximum_fusion.2), channel_id=1, source_target_pairs={{0,4},{4,8},{8,12},{12,16},{16,20},{20,24},{24,28},{28,32},{32,36}... | collective-permute-start | bytes 98312 | tf_op jit(solution)/shard_map/ppermute | solution.py:26
  15.8 0.7 copy-start.5
  16.5 0.7 copy-start.6
  17.2 7.2 %copy-start.7 = (pred[8,128,256]{1,2,0:T(8,128)(4,1)S(1)}, pred[8,128,256]{1,2,0:T(8,128)(4,1)}, u32[]{:S(2)}) copy-start(pred[8,128,256]{1,2,0:T(8,128)(4,1)} %broadcast_and_fusion) | copy-start | bytes 786436
  17.2 7.2 %copy-start.8 = (bf16[8,128,4,64]{3,2,1,0:T(4,128)(2,1)S(1)}, bf16[8,128,4,64]{3,2,1,0:T(4,128)(2,1)}, u32[]{:S(2)}) copy-start(bf16[8,128,4,64]{3,2,1,0:T(4,128)(2,1)} %reshape.135) | copy-start | bytes 1572868
  17.2 7.2 %copy-start.12 = (bf16[8,128,1,64]{1,3,0,2:T(8,128)(2,1)S(1)}, bf16[8,128,1,64]{1,3,0,2:T(8,128)(2,1)}, u32[]{:S(2)}) copy-start(bf16[8,128,1,64]{1,3,0,2:T(8,128)(2,1)} %copy.25) | copy-start | bytes 393220
  23.4 3.0 %copy-start = (bf16[8,8,2,16,512]{4,3,2,1,0:T(8,128)(2,1)}, bf16[8,8,2,16,512]{4,3,2,1,0:T(8,128)(2,1)S(1)}, u32[]{:S(2)}) copy-start(bf16[8,8,2,16,512]{4,3,2,1,0:T(8,128)(2,1)S(1)} %get-tuple-element.5.s_hbm) | copy-start | bytes 6291460
  23.4 3.0 %copy-start.3 = (f32[512,2]{1,0:T(8,128)}, f32[512,2]{1,0:T(8,128)S(1)}, u32[]{:S(2)}) copy-start(f32[512,2]{1,0:T(8,128)S(1)} %get-tuple-element.6.gates) | copy-start | bytes 12292
  23.4 3.0 %copy-start.4 = (s32[512,2]{1,0:T(8,128)}, s32[512,2]{1,0:T(8,128)S(1)}, u32[]{:S(2)}) copy-start(s32[512,2]{1,0:T(8,128)S(1)} %get-tuple-element.7.rows_in) | copy-start | bytes 12292
  23.4 1.9 copy-start.13
  24.4 2.1 %copy-start.10 = (bf16[1024,64]{0,1:T(8,128)(2,1)S(1)}, bf16[1024,64]{0,1:T(8,128)(2,1)}, u32[]{:S(2)}) copy-start(bf16[1024,64]{0,1:T(8,128)(2,1)} %param.15) | copy-start | bytes 393220
  24.4 2.2 %copy-start.11 = (bf16[8,128,1,64]{1,3,0,2:T(8,128)(2,1)S(1)}, bf16[8,128,1,64]{1,3,0,2:T(8,128)(2,1)}, u32[]{:S(2)}) copy-start(bf16[8,128,1,64]{1,3,0,2:T(8,128)(2,1)} %copy.23) | copy-start | bytes 393220

commit v2 on v1

v2 whole, which is shorter than its diff:
```python
import functools

import jax
import jax.numpy as jnp
from jax import lax
from jax.experimental import pallas as pl
from jax.experimental.pallas import tpu as pltpu
from jax.sharding import PartitionSpec as P

HEADS = 16
KV = 4
HD = 64
WINDOW = 128
CAP = 4
NTP = 4
PLANE = 8
MESH = pl.DeviceIdType.MESH
F32 = jnp.float32
BF16 = jnp.bfloat16


def hop_of(i, nz):
    if i == 0:
        return 0
    return (nz - i) // 2 if i % 2 == 0 else (i + nz - 1) // 2


def near_positions(nz):
    return [i for i in range(nz) if hop_of(i, nz) in (0, 1, nz - 1)]


def position_of(d, nz):
    return jnp.where(d == 0, 0, jnp.where(d < nz // 2, nz - 2 * d, 2 * d - nz + 1))


def slot_rows(expert, block, place, z, yc, nz, nyc):
    rank = expert >> 1
    d = ((rank >> (nyc.bit_length() - 1)) - z + nz) & (nz - 1)
    j = ((rank & (nyc - 1)) - yc + nyc) & (nyc - 1)
    return ((position_of(d, nz) * nyc + j) * 2 + (expert & 1)) * (NTP * CAP) + block * CAP + place


def iota(shape, dim):
    return lax.broadcasted_iota(jnp.int32, shape, dim)


def one_hot(hit):
    return jnp.where(hit, 1.0, 0.0).astype(BF16)


def dot_nt(a, b):
    return lax.dot_general(a, b, (((1,), (1,)), ((), ())), preferred_element_type=F32)


def step_kernel(
    nz, nyc, q_hbm, kt_hbm, vt_hbm, sink, ow_hbm, tok_hbm, gain, rgt, rex, rt, wg_hbm, wu_hbm, wd_hbm,
    mix, moe,
    tok, normed, slots, extra, relay, relay_e, arr, wg, wu, wq, act, out, back, ret, att, ow,
    fin_out, fin, gates, rows_in, qs, kvt, wide,
    zs, zr, zes, zer, ys, yr, yes, yer, xs, xr, fs, fr, acs, acr, afs, afr, ws, wr,
    rzs, rzr, rys, ryr, ts, tr, tfs, tfr, es, er, hs, hr, loc,
):
    x = lax.axis_index("tp")
    e = lax.axis_index("ep")
    z, yc = lax.div(e, nyc), lax.rem(e, nyc)
    fq = arr.shape[-1]
    hq = wg.shape[-1]
    hops = [hop_of(i, nz) for i in range(nz)]
    near = near_positions(nz)
    half = nyc // 2
    pairs = nz // 2
    tokens, width = tok.shape
    block_rows = tokens // NTP
    rest = pl.ds(1, nyc - 1)

    def zdev(d):
        return (lax.rem(z + (d + nz), nz) * nyc + yc, x)

    def ydev(j):
        return (z * nyc + lax.rem(yc + (j + nyc), nyc), x)

    def xdev(q):
        return (e, lax.rem(x + q, NTP))

    def edev(step):
        return (lax.rem(e + (step + nz * nyc), nz * nyc), x)

    def column(q):
        return lax.rem(x + (q + NTP), NTP)

    def send(src, dst, s_sem, r_sem, dev):
        copy = pltpu.make_async_remote_copy(
            src_ref=src, dst_ref=dst, send_sem=s_sem, recv_sem=r_sem,
            device_id=dev, device_id_type=MESH,
        )
        copy.start()

    def drain(ref, sem):
        pltpu.make_async_copy(ref, ref, sem).wait()

    def quarter(q, size):
        return pl.ds(pl.multiple_of(column(q) * size, size), size)

    barrier = pltpu.get_barrier_semaphore()
    peers = [xdev(q) for q in range(1, NTP)] + [edev(1), edev(-1)]
    peers += [ydev(j) for j in range(1, nyc)] + [zdev(d) for d in range(1, nz)]
    for peer in peers:
        pl.semaphore_signal(barrier, inc=1, device_id=peer, device_id_type=MESH)
    span = kt_hbm.shape[1]
    step = tokens // 4
    local = [
        pltpu.make_async_copy(wg_hbm, wg, loc.at[0]),
        pltpu.make_async_copy(wu_hbm, wu, loc.at[1]),
        pltpu.make_async_copy(wd_hbm.at[:, :, quarter(0, fq)], wq.at[0], loc.at[2]),
        pltpu.make_async_copy(ow_hbm, ow, loc.at[3]),
        pltpu.make_async_copy(q_hbm, qs, loc.at[4]),
        pltpu.make_async_copy(kt_hbm, kvt.at[0, :, pl.ds(WINDOW, span)], loc.at[5]),
        pltpu.make_async_copy(vt_hbm, kvt.at[1, :, pl.ds(WINDOW, span)], loc.at[6]),
    ]
    token_parts = [
        pltpu.make_async_copy(tok_hbm.at[pl.ds(i * step, step)], tok.at[pl.ds(i * step, step)], loc.at[7 + i])
        for i in range(4)
    ]
    for copy in token_parts + local:
        copy.start()
    pl.semaphore_wait(barrier, len(peers))

    for q in (1, 3, 2):
        send(wd_hbm.at[:, :, quarter(q, fq)], wq.at[q], ws.at[q], wr.at[q], xdev(q))
    tail = pl.ds(span - WINDOW, WINDOW)
    for w, source in enumerate((kt_hbm, vt_hbm)):
        send(source.at[:, tail], kvt.at[w, :, pl.ds(0, WINDOW)], hs.at[w], hr.at[w], edev(1))

    for i in range(4):
        token_parts[i].wait()

        def norm_rows(c, carry, i=i):
            where = pl.ds(pl.multiple_of(i * step + c * (step // 2), step // 2), step // 2)
            v = tok[where, :].astype(F32)
            ms = jnp.mean(v * v, axis=-1, keepdims=True)
            normed[where, :] = (v * lax.rsqrt(ms + 1e-06) * gain[...]).astype(BF16)
            return carry

        lax.fori_loop(0, 2, norm_rows, 0)

    experts = rex.shape[1]
    shift = block_rows.bit_length() - 1
    e0, e1 = rt[0:1, :], rt[1:2, :]
    ids = iota((experts, tokens), 0)
    hit0, hit1 = ids == e0, ids == e1
    first, second = iota((tokens, tokens), 0), iota((tokens, tokens), 1)
    before = one_hot(((first >> shift) == (second >> shift)) & (first < second))
    count = jnp.dot(one_hot(hit0 | hit1), before, preferred_element_type=F32)
    place0 = jnp.sum(jnp.where(hit0, count, 0.0), axis=0, keepdims=True).astype(jnp.int32)
    place1 = jnp.sum(jnp.where(hit1, count, 0.0), axis=0, keepdims=True).astype(jnp.int32)
    block = iota((1, tokens), 1) >> shift
    t0 = slot_rows(e0, block, place0, z, yc, nz, nyc)
    t1 = slot_rows(e1, block, place1, z, yc, nz, nyc)
    part = nyc * 2 * NTP * CAP

    def picked(i):
        ids = iota((part, tokens), 0) + i * part
        return one_hot((ids == t0) | (ids == t1))

    def filled(pick, q):
        got = jnp.dot(pick, normed[:, quarter(q, fq)], preferred_element_type=F32)
        return got.astype(BF16).reshape(nyc, 2, NTP * CAP, fq)

    def fill(i, carry):
        slots[i] = filled(picked(i), 0)
        return carry

    lax.fori_loop(0, nz, fill, 0)
    for i in range(1, nz):
        send(slots.at[i, rest], relay.at[i, rest], zs.at[i, 1], zr.at[i, 1], zdev(hops[i]))
        send(slots.at[i, 0], arr.at[0, i, 0], zs.at[i, 0], zr.at[i, 0], zdev(hops[i]))
    for j in range(1, nyc):
        send(slots.at[0, j], arr.at[0, 0, j], ys.at[0], yr.at[0], ydev(j))
    for f, i in enumerate(near):
        pick = picked(i)
        for q in range(1, NTP):
            extra[f, q - 1] = filled(pick, -q)
        for q in range(1, NTP):
            if i == 0:
                for j in range(1, nyc):
                    send(extra.at[f, q - 1, j], arr.at[q, 0, j], yes.at[f], yer.at[f], ydev(j))
                continue
            send(
                extra.at[f, q - 1, rest], relay_e.at[f, q - 1, rest],
                zes.at[f, q - 1, 1], zer.at[f, q - 1, 1], zdev(hops[i]),
            )
            send(
                extra.at[f, q - 1, 0], arr.at[q, i, 0],
                zes.at[f, q - 1, 0], zer.at[f, q - 1, 0], zdev(hops[i]),
            )
    arr[0, 0, 0] = slots[0, 0]
    for q in range(1, NTP):
        arr[q, 0, 0] = extra[0, q - 1, 0]

    lanes = iota((8, tokens), 0)
    table = jnp.zeros((8, tokens), F32)
    for at, value in enumerate((e0, e1, t0 >> 6, t0 & 63, t1 >> 6, t1 & 63)):
        table = jnp.where(lanes == at, value.astype(F32), table)
    turned = dot_nt(one_hot(first == second), table.astype(BF16)).astype(jnp.int32)
    c0, c1 = turned[:, 0:1], turned[:, 1:2]
    rows_in[:, 0:1] = turned[:, 2:3] * 64 + turned[:, 3:4]
    rows_in[:, 1:2] = turned[:, 4:5] * 64 + turned[:, 5:6]
    by_expert = jnp.dot(normed[...], rex[...], preferred_element_type=F32)
    by_group = dot_nt(normed[...], rgt[...])
    groups = rgt.shape[0]
    group_exp = jnp.exp(by_group - jnp.max(by_group, axis=1, keepdims=True))
    chosen = iota((tokens, groups), 1) == (c0 >> ((experts // groups).bit_length() - 1))
    share = jnp.sum(jnp.where(chosen, group_exp, 0.0), axis=1, keepdims=True) / jnp.sum(
        group_exp, axis=1, keepdims=True
    )
    ids = iota((tokens, experts), 1)
    l0 = jnp.sum(jnp.where(ids == c0, by_expert, 0.0), axis=1, keepdims=True)
    l1 = jnp.sum(jnp.where(ids == c1, by_expert, 0.0), axis=1, keepdims=True)
    top = jnp.maximum(l0, l1)
    x0, x1 = jnp.exp(l0 - top), jnp.exp(l1 - top)
    gates[:, 0:1] = share * (x0 / (x0 + x1))
    gates[:, 1:2] = share * (x1 / (x0 + x1))

    heads = qs.shape[1] // HD
    for copy in local[4:7]:
        copy.wait()
    for w in range(2):
        drain(kvt.at[w, :, pl.ds(0, WINDOW)], hr.at[w])
    for w in range(2):
        for h in range(heads):
            for other in range(heads):
                if other != h:
                    wide[w, h, pl.ds(other * HD, HD), :] = jnp.zeros((HD, span + WINDOW), BF16)
            wide[w, h, pl.ds(h * HD, HD), :] = kvt[w]

    def attend(b, carry):
        where = pl.ds(pl.multiple_of(b * WINDOW, WINDOW), WINDOW)
        band = pl.ds(pl.multiple_of(b * WINDOW, WINDOW), 2 * WINDOW)
        key = iota((WINDOW, 2 * WINDOW), 1)
        distance = iota((WINDOW, 2 * WINDOW), 0) + WINDOW - key
        earliest = jnp.where(e + b == 0, WINDOW, 0)
        allowed = (distance >= 0) & (distance < WINDOW) & (key >= earliest)
        queries = qs[where, :]
        total = jnp.zeros((WINDOW, heads * HD), F32)
        for h in range(heads):
            scores = jnp.dot(queries, wide[0, h, :, band], preferred_element_type=F32)
            masked = jnp.where(allowed, scores * HD ** (-0.5), -1e30)
            row_max = jnp.maximum(jnp.max(masked, axis=1, keepdims=True), sink[h])
            weights = jnp.exp(masked - row_max)
            denominator = jnp.sum(weights, axis=1, keepdims=True) + jnp.exp(sink[h] - row_max)
            probs = (weights / denominator).astype(BF16)
            total += dot_nt(probs, wide[1, h, :, band])
        att[0, where, :] = total.astype(BF16)
        return carry

    lax.fori_loop(0, span // WINDOW, attend, 0)

    def plane_out(i):
        if i == 0:
            return
        drain(relay.at[i, rest], zr.at[i, 1])
        for j in range(1, nyc):
            send(relay.at[i, j], arr.at[0, i, j], ys.at[i], yr.at[i], ydev(j))
        if i in near:
            f = near.index(i)
            for q in range(1, NTP):
                drain(relay_e.at[f, q - 1, rest], zer.at[f, q - 1, 1])
                for j in range(1, nyc):
                    send(relay_e.at[f, q - 1, j], arr.at[q, i, j], yes.at[f], yer.at[f], ydev(j))

    def ring_own(i):
        if i > 0:
            drain(arr.at[0, i, 0], zr.at[i, 0])
        drain(arr.at[0, i, rest], yr.at[i])
        if i in near:
            return
        send(arr.at[0, i], arr.at[1, i], xs.at[i, 0], xr.at[i, 0], xdev(1))
        send(arr.at[0, i], arr.at[3, i], xs.at[i, 1], xr.at[i, 1], xdev(3))

    low, high = pl.ds(0, half), pl.ds(half, half)

    def ring_on(i):
        if i in near:
            return
        drain(arr.at[1, i], xr.at[i, 0])
        send(arr.at[1, i, low], arr.at[2, i, low], fs.at[i, 0], fr.at[i, 0], xdev(1))
        drain(arr.at[3, i], xr.at[i, 1])
        send(arr.at[3, i, high], arr.at[2, i, high], fs.at[i, 1], fr.at[i, 1], xdev(3))

    def ring_in(i):
        if i in near:
            f = near.index(i)
            if i > 0:
                for q in range(1, NTP):
                    drain(arr.at[q, i, 0], zer.at[f, q - 1, 0])
            drain(arr.at[pl.ds(1, NTP - 1), i, rest], yer.at[f])
            return
        drain(arr.at[2, i, low], fr.at[i, 0])
        drain(arr.at[2, i, high], fr.at[i, 1])

    rows2 = 2 * nyc * NTP * CAP

    def hidden(p):
        if p == 0:
            local[0].wait()
            local[1].wait()

        def one(k, carry):
            gate = jnp.zeros((rows2, hq), F32)
            up = jnp.zeros((rows2, hq), F32)
            for q in range(NTP):
                depth = quarter(-q, fq)
                rows = arr[q, pl.ds(2 * p, 2), :, k].reshape(rows2, fq)
                gate += jnp.dot(rows, wg[k, depth, :], preferred_element_type=F32)
                up += jnp.dot(rows, wu[k, depth, :], preferred_element_type=F32)
            act[0, p, k] = (gate / (1.0 + jnp.exp(-gate)) * up).astype(BF16)
            return carry

        lax.fori_loop(0, 2, one, 0)
        send(act.at[0, p], act.at[1, p], acs.at[p, 0], acr.at[p, 0], xdev(1))
        send(act.at[0, p], act.at[3, p], acs.at[p, 1], acr.at[p, 1], xdev(3))

    def act_on(p):
        drain(act.at[1, p], acr.at[p, 0])
        send(act.at[1, p, 0], act.at[2, p, 0], afs.at[p, 0], afr.at[p, 0], xdev(1))
        drain(act.at[3, p], acr.at[p, 1])
        send(act.at[3, p, 1], act.at[2, p, 1], afs.at[p, 1], afr.at[p, 1], xdev(3))

    def down(p):
        if p == 0:
            local[2].wait()
            for q in range(1, NTP):
                drain(wq.at[q], wr.at[q])
        drain(act.at[2, p, 0], afr.at[p, 0])
        drain(act.at[2, p, 1], afr.at[p, 1])

        def one(k, carry):
            total = jnp.zeros((rows2, fq), F32)
            for q in range(NTP):
                total += jnp.dot(act[q, p, k], wq[q, k], preferred_element_type=F32)
            out[pl.ds(2 * p, 2), :, k] = total.astype(BF16).reshape(2, nyc, NTP * CAP, fq)
            return carry

        lax.fori_loop(0, 2, one, 0)
        for i in (2 * p, 2 * p + 1):
            if i == 0:
                ret[0, 0] = out[0, 0]
                for j in range(1, nyc):
                    send(out.at[0, j], ret.at[0, j], rys.at[0], ryr.at[0], ydev(-j))
                continue
            send(out.at[i, rest], back.at[i, rest], rzs.at[i, 1], rzr.at[i, 1], zdev(-hops[i]))
            send(out.at[i, 0], ret.at[i, 0], rzs.at[i, 0], rzr.at[i, 0], zdev(-hops[i]))

    def plane_back(i):
        if i == 0:
            return
        drain(back.at[i, rest], rzr.at[i, 1])
        for j in range(1, nyc):
            send(back.at[i, j], ret.at[i, j], rys.at[i], ryr.at[i], ydev(-j))

    for n in range(nz + 2):
        if n < nz:
            plane_out(n)
        if 0 <= n - 1 < nz:
            ring_own(n - 1)
        if 0 <= n - 2 < nz:
            ring_on(n - 2)
        m = n - 3
        if m >= 0:
            ring_in(m)
            if m % 2 == 1:
                hidden(m // 2)
                if m >= 3:
                    down(m // 2 - 1)
            elif m >= 2:
                act_on(m // 2 - 1)
    ring_in(nz - 1)
    hidden(pairs - 1)
    if pairs > 1:
        down(pairs - 2)
    act_on(pairs - 1)
    rows = att.shape[1]
    top, bottom = pl.ds(0, rows // 2), pl.ds(rows // 2, rows // 2)
    send(att.at[0], att.at[1], ts.at[0], tr.at[0], xdev(1))
    send(att.at[0], att.at[3], ts.at[1], tr.at[1], xdev(3))
    for i in range(nz - 4):
        plane_back(i)
    down(pairs - 1)
    for i in range(max(nz - 4, 0), nz - 2):
        plane_back(i)
    drain(att.at[1], tr.at[0])
    send(att.at[1, top], att.at[2, top], tfs.at[0], tfr.at[0], xdev(1))
    drain(att.at[3], tr.at[1])
    send(att.at[3, bottom], att.at[2, bottom], tfs.at[1], tfr.at[1], xdev(3))
    for i in range(nz - 2, nz):
        plane_back(i)
    local[3].wait()
    drain(att.at[2, top], tfr.at[0])
    drain(att.at[2, bottom], tfr.at[1])
    chunk = rows // 4
    hw = att.shape[2]

    def project(c, carry):
        where = pl.ds(pl.multiple_of(c * chunk, chunk), chunk)
        total = jnp.zeros((chunk, ow.shape[1]), F32)
        for q in range(NTP):
            total += jnp.dot(att[q, where, :], ow[quarter(-q, hw), :], preferred_element_type=F32)
        mix[where, :] = total.astype(BF16)
        return carry

    lax.fori_loop(0, 4, project, 0)

    for i in range(nz):
        if i > 0:
            drain(ret.at[i, 0], rzr.at[i, 0])
        drain(ret.at[i, rest], ryr.at[i])

    total_slots = nz * nyc * 2 * NTP * CAP

    def combined(t):
        where = pl.ds(pl.multiple_of(t * block_rows, block_rows), block_rows)
        ids = iota((block_rows, total_slots), 1)
        at = rows_in[where, :]
        pick = jnp.concatenate([one_hot(ids == at[:, k : k + 1]) for k in range(2)], axis=0)
        got = jnp.dot(pick, ret[...].reshape(total_slots, fq), preferred_element_type=F32)
        g = gates[where, :]
        return (g[:, 0:1] * got[:block_rows] + g[:, 1:2] * got[block_rows:]).astype(BF16)

    for q in (2, 1, 3):
        fin_out[q] = combined(column(q))
        send(fin_out.at[q], fin.at[q], es.at[q], er.at[q], xdev(q))
    moe[:, quarter(0, fq)] = combined(x)
    for q in range(1, NTP):
        drain(fin.at[q], er.at[q])
        moe[:, quarter(-q, fq)] = fin[q]

    for i in range(nz):
        if i > 0:
            drain(relay.at[i, 0], zs.at[i, 0])
            drain(relay.at[i, rest], zs.at[i, 1])
            drain(out.at[i, 0], rzs.at[i, 0])
            drain(out.at[i, rest], rzs.at[i, 1])
        drain(arr.at[0, i, rest], ys.at[i])
        drain(ret.at[i, rest], rys.at[i])
        if i in near:
            f = near.index(i)
            drain(arr.at[pl.ds(1, NTP - 1), i, rest], yes.at[f])
            if i > 0:
                for q in range(NTP - 1):
                    drain(relay.at[i, 0], zes.at[f, q, 0])
                    drain(relay.at[i, rest], zes.at[f, q, 1])
            continue
        for way in range(2):
            drain(arr.at[0, i], xs.at[i, way])
            drain(arr.at[0, i, low], fs.at[i, way])
    for p in range(pairs):
        for way in range(2):
            drain(act.at[0, p], acs.at[p, way])
            drain(act.at[0, p, 0], afs.at[p, way])
    for way in range(2):
        drain(att.at[0], ts.at[way])
        drain(att.at[0, top], tfs.at[way])
        drain(kvt.at[way, :, pl.ds(0, WINDOW)], hs.at[way])
    for q in range(1, NTP):
        drain(wq.at[q], ws.at[q])
        drain(fin_out.at[q], es.at[q])


def per_device(
    q_heads,
    k_heads,
    v_heads,
    sink_logits,
    out_weight,
    tokens_b,
    moe_gain,
    router_group,
    router_expert,
    route_expert,
    expert_gate,
    expert_up,
    expert_down,
):
    nyc = min(PLANE, lax.axis_size("ep"))
    nz = lax.axis_size("ep") // nyc
    tokens, width = tokens_b.shape
    fq = width // NTP
    hq = expert_gate.shape[2]
    sixteen = NTP * CAP
    span = q_heads.shape[0]
    vmem = pl.BlockSpec(memory_space=pltpu.VMEM)
    smem = pl.BlockSpec(memory_space=pltpu.SMEM)
    anywhere = pl.BlockSpec(memory_space=pl.ANY)
    dma = pltpu.SemaphoreType.DMA
    pairs = nz // 2
    near = len(near_positions(nz))
    rows2 = 2 * nyc * sixteen
    slot = (nz, nyc, 2, sixteen, fq)
    more = (near, NTP - 1, nyc, 2, sixteen, fq)
    return pl.pallas_call(
        functools.partial(step_kernel, nz, nyc),
        out_shape=(
            jax.ShapeDtypeStruct((span, out_weight.shape[1]), BF16),
            jax.ShapeDtypeStruct((tokens // NTP, width), BF16),
        ),
        in_specs=[anywhere] * 3 + [smem] + [anywhere] * 2 + [vmem] * 4 + [anywhere] * 3,
        out_specs=(vmem, vmem),
        scratch_shapes=[
            pltpu.VMEM(tokens_b.shape, BF16),
            pltpu.VMEM(tokens_b.shape, BF16),
            pltpu.VMEM(slot, BF16),
            pltpu.VMEM(more, BF16),
            pltpu.VMEM(slot, BF16),
            pltpu.VMEM(more, BF16),
            pltpu.VMEM((NTP, *slot), BF16),
            pltpu.VMEM(expert_gate.shape, BF16),
            pltpu.VMEM(expert_up.shape, BF16),
            pltpu.VMEM((NTP, 2, hq, fq), BF16),
            pltpu.VMEM((NTP, pairs, 2, rows2, hq), BF16),
            pltpu.VMEM(slot, BF16),
            pltpu.VMEM(slot, BF16),
            pltpu.VMEM(slot, BF16),
            pltpu.VMEM((NTP, *q_heads.shape), BF16),
            pltpu.VMEM(out_weight.shape, BF16),
            pltpu.VMEM((NTP, tokens // NTP, fq), BF16),
            pltpu.VMEM((NTP, tokens // NTP, fq), BF16),
            pltpu.VMEM((tokens, 2), F32),
            pltpu.VMEM((tokens, 2), jnp.int32),
            pltpu.VMEM(q_heads.shape, BF16),
            pltpu.VMEM((2, HD, span + WINDOW), BF16),
            pltpu.VMEM((2, q_heads.shape[1] // HD, q_heads.shape[1], span + WINDOW), BF16),
            dma((nz, 2)), dma((nz, 2)), dma((near, NTP - 1, 2)), dma((near, NTP - 1, 2)),
            dma((nz,)), dma((nz,)), dma((near,)), dma((near,)),
            dma((nz, 2)), dma((nz, 2)), dma((nz, 2)), dma((nz, 2)),
            dma((pairs, 2)), dma((pairs, 2)), dma((pairs, 2)), dma((pairs, 2)),
            dma((NTP,)), dma((NTP,)),
            dma((nz, 2)), dma((nz, 2)), dma((nz,)), dma((nz,)),
            dma((2,)), dma((2,)), dma((2,)), dma((2,)),
            dma((NTP,)), dma((NTP,)), dma((2,)), dma((2,)), dma((11,)),
        ],
        compiler_params=pltpu.CompilerParams(
            collective_id=0, has_side_effects=True, vmem_limit_bytes=62 * 2**20
        ),
        name="step",
    )(
        q_heads,
        k_heads.T,
        v_heads.T,
        sink_logits,
        out_weight,
        tokens_b,
        moe_gain.reshape(1, width),
        router_group.T,
        router_expert,
        route_expert.T,
        expert_gate,
        expert_up,
        expert_down,
    )


def solution(mesh):
    in_specs = (
        P("ep", "tp"),
        P("ep", "tp"),
        P("ep", "tp"),
        P("tp"),
        P(None, "tp"),
        P("ep", None),
        P(),
        P(),
        P(),
        P("ep", None),
        P("ep", None, "tp"),
        P("ep", None, "tp"),
        P("ep", "tp", None),
    )
    out_specs = (P("ep", "tp"), P(("ep", "tp"), None))
    return jax.shard_map(
        per_device, mesh=mesh, in_specs=in_specs, out_specs=out_specs, check_vma=False
    )
```

time: 205 us -> 166 us (0.81)
  Pallas kernels: 177 us -> 162 us
  local copies, waits for them, and re-layouts: 17.3 us -> 3.12 us
  starting transfers between devices: 4.57 us -> 0 us
  other arithmetic: 2.98 us -> 0 us
  matrix products: 2.1 us -> 0 us
    pallas_call x2 -> x1, Pallas kernels: 177 us -> 162 us  [per_device(): pl.pallas_call(functools.partial(step_kernel, nz, nyc), out_shape=(jax.Sh...]
    unnamed x36 -> x4, local copies, waits for them, and re-layouts: 9.32 us -> 3.12 us
    ppermute x1 -> x0, starting transfers between devices: 4.57 us -> none  [shifted(): lax.ppermute(value, axis, [(source, source + steps) for source in range(l...]
    another operation x2 -> x0, local copies, waits for them, and re-layouts: 3.65 us -> none
    reshape x2 -> x0, local copies, waits for them, and re-layouts: 2.15 us -> none  [attention(): attended.astype(jnp.bfloat16).reshape(row_count, kv_local * group_size * HD)]
    dot_general x2 -> x0, matrix products: 2.1 us -> none  [the longest x1 1.2 us: attention(): jnp.einsum('nhgqk,nkhd->nqhgd', probs, value_band, preferred_element_type...]
  transfers between devices with their start and end apart: 1 -> 0, of which waited for: 0 -> 0; matrix products, arithmetic and copies ran while one was open for 4% -> 0% of each run, Pallas kernels for 3% -> 0%
where the time goes in v2:
time: 166 us
  Pallas kernels  162 us (98%)
  local copies, waits for them, and re-layouts  3.12 us (2%)
    pallas_call x1, Pallas kernels, per_device(): pl.pallas_call(functools.partial(step_kernel, nz, nyc), out_shape=(jax.Sh...  162 us

profile of v2, /device:TPU:1, one launch (start us, length us, event | category | flops | bytes accessed | tf_op | source)
XLA Modules:
  0.0 166.2 jit_solution(1587484170682805014)
XLA Ops:
  0.6 162.4 %step.1 = (bf16[1024,512]{1,0:T(8,128)(2,1)}, bf16[128,2048]{1,0:T(8,128)(2,1)}) custom-call(bf16[1024,256]{1,0:T(8,128)(2,1)} %q_hbm.1, bf16[64,1024]{1,0:T(8,128)(2,1)} %bitcast.5, bf16[64,1024]{1,0:T(8,128)(2,1)} %bitcast.6, f32[4]{0:T(128)} %sink.1, bf16[1024,512]{1,0:T(8,128)(2,1)} %ow_hbm.1, bf16[512,2048]{1,0:T(8,128)(2,1)} %tok_hbm.1, ...), custom_call_target="tpu_custom_call" | custom-call | tf_op jit(solution)/shard_map/step/pallas_call | solution.py:500
  163.1 0.0 copy-start
  163.1 2.3 %copy.17 = bf16[1024,512]{1,0:T(8,128)(2,1)} copy(bf16[1024,512]{1,0:T(8,128)(2,1)} %get-tuple-element.4) | data formatting | bytes 2097152
  165.4 0.0 copy-done
  165.4 0.8 copy.18
Async XLA Ops:
  163.1 2.3 %copy-start = (bf16[128,2048]{1,0:T(8,128)(2,1)S(1)}, bf16[128,2048]{1,0:T(8,128)(2,1)}, u32[]{:S(2)}) copy-start(bf16[128,2048]{1,0:T(8,128)(2,1)} %get-tuple-element.5) | copy-start | bytes 1572868

commit v3 on v2

v3 whole, which is shorter than its diff:
```python
import functools

import jax
import jax.numpy as jnp
from jax import lax
from jax.experimental import pallas as pl
from jax.experimental.pallas import tpu as pltpu
from jax.sharding import PartitionSpec as P

HEADS = 16
KV = 4
HD = 64
WINDOW = 128
CAP = 4
NTP = 4
PLANE = 8
GROUPS = 4
NEAR = (0, 1, 7)
TWO = (2, 6)
MESSAGES = [(1, 0), (2, 0), (3, 0), (4, 0), (5, 0), (4, 2), (5, 2), (6, 0), (7, 0)]
CHUNKS = [(1, 2), (3, 1), (4, 2), (6, 2), (0, 1)]
MIDDLE = (
    "Z0", "Z1", "O1", "Z2", "O2", "Z-1", "O3", "Z3", "F1", "Z4", "Z5", "Z6", "F2", "F3", "O4", "Z7",
    "I1", "I2", "H0", "Z8", "I3", "H1", "O5", "A0", "A1", "I4", "I5", "H2", "D0", "D1", "I6", "I7",
    "H3", "A2", "I0", "H4", "B1", "B2", "B3", "A3", "D2", "A4", "T0", "D3", "B4", "B5",
)
TAIL = (
    "D4", "B6", "B7", "B0", "T1",
)
AHEAD = 2
MESH = pl.DeviceIdType.MESH
F32 = jnp.float32
BF16 = jnp.bfloat16


def hop_of(i, nz):
    return ([0, 3, 5, 4, 2, 6, 1, 7])[i] if nz == 8 else i


def near_positions(nz):
    return [i for i in range(nz) if hop_of(i, nz) in NEAR]


def plain_chunks(nz):
    return [(2 * p, 2) for p in range(nz // 2)]


def slot_entries(nz):
    near = near_positions(nz)
    kinds = [range(NTP) if i in near else (0, 2) if hop_of(i, nz) in TWO else (0,) for i in range(nz)]
    return [(i, q) for i in range(nz) for q in kinds[i]]


def plain_messages(far, two, near):
    return [(i, 0) for i in far] + [(i, 2) for i in two] + [(i, 0) for i in near if i > 0]


def plain_order(messages, far, two, nz):
    steps = [f"Z{k}" for k in range(len(messages))] + [f"O{i}" for i in far]
    steps += [f"F{i}" for i in far if i not in two]
    steps += [f"I{i}" for i in range(nz)]
    for p in range(nz // 2):
        steps += [f"H{p}", f"A{p}"]
        if p < nz // 2 - 1:
            steps += [f"D{p}", f"B{2 * p}", f"B{2 * p + 1}"]
    return steps


def iota(shape, dim):
    return lax.broadcasted_iota(jnp.int32, shape, dim)


def one_hot(hit):
    return jnp.where(hit, 1.0, 0.0).astype(BF16)


def dot_nt(a, b):
    return lax.dot_general(a, b, (((1,), (1,)), ((), ())), preferred_element_type=F32)


def step_kernel(
    nz, nyc, q_hbm, kt_hbm, vt_hbm, sink, ow_hbm, tok_hbm, gain_hbm, rgt_hbm, rex_hbm, rt_hbm,
    wg_hbm, wu_hbm, wd_hbm, mix_hbm, moe,
    gain, rgt, rex, rt, mix,
    tok, normed, comp, meta, order, cin, cin_e, min_, mcol, relay, arr, wg, wu, wq, act,
    out, back, pout, rtok, att, ow, fin_out, fin, qs, kvt, wide,
    zs, zr, ms, mr, ys, yr, yes, yer, xs, xr, fs, fr, acs, acr, afs, afr, ws, wr,
    rzs, rzr, rys, ryr, ts, tr, tfs, tfr, es, er, hs, hr, loc,
):
    x = lax.axis_index("tp")
    e = lax.axis_index("ep")
    z, yc = lax.div(e, nyc), lax.rem(e, nyc)
    fq = arr.shape[-1]
    hq = wg.shape[-1]
    hops = [hop_of(i, nz) for i in range(nz)]
    near = near_positions(nz)
    half = nyc // 2
    chunks = CHUNKS if nz == 8 else plain_chunks(nz)
    tokens, width = tok.shape
    block_rows = tokens // NTP
    rest = pl.ds(1, nyc - 1)

    def zdev(d):
        return (lax.rem(z + (d + nz), nz) * nyc + yc, x)

    def ydev(j):
        return (z * nyc + lax.rem(yc + (j + nyc), nyc), x)

    def xdev(q):
        return (e, lax.rem(x + q, NTP))

    def edev(step):
        return (lax.rem(e + (step + nz * nyc), nz * nyc), x)

    def column(q):
        return lax.rem(x + (q + NTP), NTP)

    def send(src, dst, s_sem, r_sem, dev):
        copy = pltpu.make_async_remote_copy(
            src_ref=src, dst_ref=dst, send_sem=s_sem, recv_sem=r_sem,
            device_id=dev, device_id_type=MESH,
        )
        copy.start()

    def drain(ref, sem):
        pltpu.make_async_copy(ref, ref, sem).wait()

    def quarter(q, size):
        return pl.ds(pl.multiple_of(column(q) * size, size), size)

    barrier = pltpu.get_barrier_semaphore()
    peers = [xdev(q) for q in range(1, NTP)] + [edev(1), edev(-1)]
    peers += [ydev(j) for j in range(1, nyc)] + [zdev(d) for d in range(1, nz)]
    for peer in peers:
        pl.semaphore_signal(barrier, inc=1, device_id=peer, device_id_type=MESH)
    span = kt_hbm.shape[1]
    step = tokens // 4
    local = [
        pltpu.make_async_copy(wg_hbm, wg, loc.at[0]),
        pltpu.make_async_copy(wu_hbm, wu, loc.at[1]),
        pltpu.make_async_copy(wd_hbm.at[:, :, quarter(0, fq)], wq.at[0], loc.at[2]),
        pltpu.make_async_copy(ow_hbm, ow, loc.at[3]),
        pltpu.make_async_copy(q_hbm, qs, loc.at[4]),
        pltpu.make_async_copy(kt_hbm, kvt.at[0, :, pl.ds(WINDOW, span)], loc.at[5]),
        pltpu.make_async_copy(vt_hbm, kvt.at[1, :, pl.ds(WINDOW, span)], loc.at[6]),
    ]
    token_parts = [
        pltpu.make_async_copy(tok_hbm.at[pl.ds(i * step, step)], tok.at[pl.ds(i * step, step)], loc.at[7 + i])
        for i in range(4)
    ]
    small = [
        pltpu.make_async_copy(source, target, loc.at[11 + n])
        for n, (source, target) in enumerate(
            ((gain_hbm, gain), (rt_hbm, rt), (rgt_hbm, rgt), (rex_hbm, rex))
        )
    ]
    for copy in token_parts + small + local:
        copy.start()
    pl.semaphore_wait(barrier, len(peers))

    for q in (1, 3, 2):
        send(wd_hbm.at[:, :, quarter(q, fq)], wq.at[q], ws.at[q], wr.at[q], xdev(q))
    tail = pl.ds(span - WINDOW, WINDOW)
    for w, source in enumerate((kt_hbm, vt_hbm)):
        send(source.at[:, tail], kvt.at[w, :, pl.ds(0, WINDOW)], hs.at[w], hr.at[w], edev(1))

    for copy in small:
        copy.wait()
    for i in range(4):
        token_parts[i].wait()

        def norm_rows(c, carry, i=i):
            where = pl.ds(pl.multiple_of(i * step + c * (step // 2), step // 2), step // 2)
            v = tok[where, :].astype(F32)
            ms = jnp.mean(v * v, axis=-1, keepdims=True)
            normed[where, :] = (v * lax.rsqrt(ms + 1e-06) * gain[...]).astype(BF16)
            return carry

        lax.fori_loop(0, 2, norm_rows, 0)

    experts = rex.shape[1]
    shift = block_rows.bit_length() - 1
    per_group = block_rows // GROUPS
    group_rows = tokens // GROUPS
    planes = nz // GROUPS
    part = nyc * 2 * NTP * CAP
    e0, e1 = rt[0:1, :], rt[1:2, :]
    ids = iota((experts, tokens), 0)
    hit0, hit1 = ids == e0, ids == e1
    first, second = iota((tokens, tokens), 0), iota((tokens, tokens), 1)
    before = one_hot(((first >> shift) == (second >> shift)) & (first < second))
    count = jnp.dot(one_hot(hit0 | hit1), before, preferred_element_type=F32)
    place0 = jnp.sum(jnp.where(hit0, count, 0.0), axis=0, keepdims=True).astype(jnp.int32)
    place1 = jnp.sum(jnp.where(hit1, count, 0.0), axis=0, keepdims=True).astype(jnp.int32)
    group = e0 >> ((experts // GROUPS).bit_length() - 1)
    mine = iota((16, tokens), 0) == group
    count = jnp.dot(one_hot(mine), before, preferred_element_type=F32)
    nth = jnp.sum(jnp.where(mine, count, 0.0), axis=0, keepdims=True).astype(jnp.int32)
    block = iota((1, tokens), 1) >> shift
    in_block = group * per_group + nth
    place = group * group_rows + block * per_group + nth

    def compact(c, carry):
        where = pl.ds(pl.multiple_of(c * group_rows, group_rows), group_rows)
        pick = one_hot(iota((group_rows, tokens), 0) + c * group_rows == place)
        comp[where, :] = jnp.dot(pick, normed[...], preferred_element_type=F32).astype(BF16)
        return carry

    lax.fori_loop(0, GROUPS, compact, 0)

    def group_at(d):
        g = lax.div(lax.rem(z + (d + nz), nz), planes)
        return pl.ds(pl.multiple_of(g * group_rows, group_rows), group_rows)

    far = [i for i in range(nz) if i not in near]
    two = [i for i in far if hops[i] in TWO]
    messages = MESSAGES if nz == 8 else plain_messages(far, two, near)
    entries = slot_entries(nz)

    def plane_send(k):
        i, q = messages[k]
        if i in near:
            source, target = comp.at[group_at(hops[i]), :], cin_e.at[near.index(i)]
        else:
            source, target = comp.at[group_at(hops[i]), quarter(-q, fq)], cin.at[i, q // 2]
        send(source, target, zs.at[k], zr.at[k], zdev(hops[i]))

    for k in range(min(AHEAD, len(messages))):
        plane_send(k)

    by_expert = lax.dot_general(
        rex[...], normed[...], (((0,), (1,)), ((), ())), preferred_element_type=F32
    )
    by_group = dot_nt(rgt[...], normed[...])
    groups = rgt.shape[0]
    group_exp = jnp.exp(by_group - jnp.max(by_group, axis=0, keepdims=True))
    chosen = iota((groups, tokens), 0) == group
    share = jnp.sum(jnp.where(chosen, group_exp, 0.0), axis=0, keepdims=True) / jnp.sum(
        group_exp, axis=0, keepdims=True
    )
    l0 = jnp.sum(jnp.where(hit0, by_expert, 0.0), axis=0, keepdims=True)
    l1 = jnp.sum(jnp.where(hit1, by_expert, 0.0), axis=0, keepdims=True)
    top = jnp.maximum(l0, l1)
    x0, x1 = jnp.exp(l0 - top), jnp.exp(l1 - top)

    def plane_row(expert, place):
        j = (((expert >> 1) & (nyc - 1)) - yc + nyc) & (nyc - 1)
        return (j * 2 + (expert & 1)) * (NTP * CAP) + block * CAP + place

    def plane_of(expert):
        return expert >> nyc.bit_length()

    def pieces(value):
        high = value.astype(BF16).astype(F32)
        middle = (value - high).astype(BF16).astype(F32)
        return (high, middle, value - high - middle)

    values = [plane_row(e0, place0), plane_row(e1, place1), plane_of(e0), plane_of(e1)]
    values += [*pieces(share * (x0 / (x0 + x1))), *pieces(share * (x1 / (x0 + x1)))]
    lanes = iota((16, tokens), 0)
    table = jnp.zeros((16, tokens), F32)
    for at, value in enumerate(values):
        table = jnp.where(lanes == at, value.astype(F32), table)
    spread = one_hot(first == place)
    turned = dot_nt(table.astype(BF16), spread)
    for g in range(GROUPS):
        meta[g] = turned[:, g * group_rows : (g + 1) * group_rows]
    order[...] = jnp.broadcast_to(in_block.astype(F32), order.shape)
    for i in range(1, nz):
        g = lax.div(lax.rem(z + (hops[i] + nz), nz), planes)
        send(meta.at[g], min_.at[i], ms.at[i], mr.at[i], zdev(hops[i]))
    min_[0] = meta[lax.div(z, planes)]

    eye = one_hot(iota((group_rows, group_rows), 0) == iota((group_rows, group_rows), 1))

    def plane_out(k):
        i, first_q = (0, 0) if k < 0 else messages[k]
        if i > 0:
            drain(cin_e.at[near.index(i)] if i in near else cin.at[i, first_q // 2], zr.at[k])
            if k + AHEAD < len(messages):
                plane_send(k + AHEAD)
            if first_q == 0:
                drain(min_.at[i], mr.at[i])
        given = min_[i]
        if first_q == 0:
            mcol[i] = dot_nt(eye, given.astype(BF16))
        row0 = jnp.where(given[2:3, :].astype(jnp.int32) == z, given[0:1, :].astype(jnp.int32), -1)
        row1 = jnp.where(given[3:4, :].astype(jnp.int32) == z, given[1:2, :].astype(jnp.int32), -1)
        ids = iota((part, group_rows), 0)
        pick = one_hot((ids == row0) | (ids == row1))
        for q in range(NTP) if i in near else (first_q,):
            if i == 0:
                rows = comp[group_at(0), quarter(-q, fq)]
            elif i in near:
                rows = cin_e[near.index(i), :, quarter(-q, fq)]
            else:
                rows = cin[i, q // 2]
            got = jnp.dot(pick, rows, preferred_element_type=F32).astype(BF16)
            got = got.reshape(nyc, 2, NTP * CAP, fq)
            at = entries.index((i, q))
            arr[q, i, 0] = got[0]
            relay[at, rest] = got[1:]
            for j in range(1, nyc):
                if q == 0:
                    send(relay.at[at, j], arr.at[0, i, j], ys.at[i], yr.at[i], ydev(j))
                else:
                    send(relay.at[at, j], arr.at[q, i, j], yes.at[i], yer.at[i], ydev(j))

    def others(i):
        if i in near:
            return arr.at[pl.ds(1, NTP - 1), i, rest]
        return arr.at[2, i, rest]

    heads = qs.shape[1] // HD
    for copy in local[4:7]:
        copy.wait()
    for w in range(2):
        drain(kvt.at[w, :, pl.ds(0, WINDOW)], hr.at[w])
    for w in range(2):
        for h in range(heads):
            for other in range(heads):
                if other != h:
                    wide[w, h, pl.ds(other * HD, HD), :] = jnp.zeros((HD, span + WINDOW), BF16)
            wide[w, h, pl.ds(h * HD, HD), :] = kvt[w]

    def attend(b, carry):
        where = pl.ds(pl.multiple_of(b * WINDOW, WINDOW), WINDOW)
        band = pl.ds(pl.multiple_of(b * WINDOW, WINDOW), 2 * WINDOW)
        key = iota((WINDOW, 2 * WINDOW), 1)
        distance = iota((WINDOW, 2 * WINDOW), 0) + WINDOW - key
        earliest = jnp.where(e + b == 0, WINDOW, 0)
        allowed = (distance >= 0) & (distance < WINDOW) & (key >= earliest)
        queries = qs[where, :]
        total = jnp.zeros((WINDOW, heads * HD), F32)
        for h in range(heads):
            scores = jnp.dot(queries, wide[0, h, :, band], preferred_element_type=F32)
            masked = jnp.where(allowed, scores * HD ** (-0.5), -1e30)
            row_max = jnp.maximum(jnp.max(masked, axis=1, keepdims=True), sink[h])
            weights = jnp.exp(masked - row_max)
            denominator = jnp.sum(weights, axis=1, keepdims=True) + jnp.exp(sink[h] - row_max)
            probs = (weights / denominator).astype(BF16)
            total += dot_nt(probs, wide[1, h, :, band])
        att[0, where, :] = total.astype(BF16)
        return carry

    lax.fori_loop(0, span // WINDOW, attend, 0)

    def ring_own(i):
        drain(arr.at[0, i, rest], yr.at[i])
        send(arr.at[0, i], arr.at[1, i], xs.at[i, 0], xr.at[i, 0], xdev(1))
        send(arr.at[0, i], arr.at[3, i], xs.at[i, 1], xr.at[i, 1], xdev(3))

    low, high = pl.ds(0, half), pl.ds(half, half)

    def ring_on(i):
        drain(arr.at[1, i], xr.at[i, 0])
        send(arr.at[1, i, low], arr.at[2, i, low], fs.at[i, 0], fr.at[i, 0], xdev(1))
        drain(arr.at[3, i], xr.at[i, 1])
        send(arr.at[3, i, high], arr.at[2, i, high], fs.at[i, 1], fr.at[i, 1], xdev(3))

    def ring_in(i):
        if i in near:
            drain(arr.at[0, i, rest], yr.at[i])
        elif i in two:
            drain(arr.at[1, i], xr.at[i, 0])
            drain(arr.at[3, i], xr.at[i, 1])
        else:
            drain(arr.at[2, i, low], fr.at[i, 0])
            drain(arr.at[2, i, high], fr.at[i, 1])
            return
        drain(others(i), yer.at[i])

    rows1 = nyc * NTP * CAP

    def span_of(c):
        first, many = chunks[c]
        return pl.ds(first, many), many * rows1

    def hidden(c):
        if c == 0:
            local[0].wait()
            local[1].wait()
        span, rows2 = span_of(c)

        def one(k, carry):
            gate = jnp.zeros((rows2, hq), F32)
            up = jnp.zeros((rows2, hq), F32)
            for q in range(NTP):
                depth = quarter(-q, fq)
                rows = arr[q, span, :, k].reshape(rows2, fq)
                gate += jnp.dot(rows, wg[k, depth, :], preferred_element_type=F32)
                up += jnp.dot(rows, wu[k, depth, :], preferred_element_type=F32)
            value = (gate / (1.0 + jnp.exp(-gate)) * up).astype(BF16)
            act[0, span, k] = value.reshape(-1, rows1, hq)
            return carry

        lax.fori_loop(0, 2, one, 0)
        send(act.at[0, span], act.at[1, span], acs.at[c, 0], acr.at[c, 0], xdev(1))
        send(act.at[0, span], act.at[3, span], acs.at[c, 1], acr.at[c, 1], xdev(3))

    def act_on(c):
        span, _ = span_of(c)
        drain(act.at[1, span], acr.at[c, 0])
        send(act.at[1, span, 0], act.at[2, span, 0], afs.at[c, 0], afr.at[c, 0], xdev(1))
        drain(act.at[3, span], acr.at[c, 1])
        send(act.at[3, span, 1], act.at[2, span, 1], afs.at[c, 1], afr.at[c, 1], xdev(3))

    def down(c):
        if c == 0:
            local[2].wait()
            for q in range(1, NTP):
                drain(wq.at[q], wr.at[q])
        span, rows2 = span_of(c)
        drain(act.at[2, span, 0], afr.at[c, 0])
        drain(act.at[2, span, 1], afr.at[c, 1])

        def one(k, carry):
            total = jnp.zeros((rows2, fq), F32)
            for q in range(NTP):
                rows = act[q, span, k].reshape(rows2, hq)
                total += jnp.dot(rows, wq[q, k], preferred_element_type=F32)
            out[span, :, k] = total.astype(BF16).reshape(-1, nyc, NTP * CAP, fq)
            return carry

        lax.fori_loop(0, 2, one, 0)
        for i in range(chunks[c][0], sum(chunks[c])):
            for j in range(1, nyc):
                send(out.at[i, j], back.at[i, j], rys.at[i], ryr.at[i], ydev(-j))
            back[i, 0] = out[i, 0]

    def plane_back(i):
        drain(back.at[i, rest], ryr.at[i])
        given = mcol[i]
        ids = iota((group_rows, part), 1)
        picks = []
        for k in range(2):
            row = given[:, k : k + 1].astype(jnp.int32)
            here = given[:, 2 + k : 3 + k].astype(jnp.int32) == z
            picks.append(one_hot(ids == jnp.where(here, row, -1)))
        got = jnp.dot(
            jnp.concatenate(picks, axis=0), back[i].reshape(part, fq), preferred_element_type=F32
        )
        g0 = given[:, 4:5] + given[:, 5:6] + given[:, 6:7]
        g1 = given[:, 7:8] + given[:, 8:9] + given[:, 9:10]
        total = (g0 * got[:group_rows] + g1 * got[group_rows:]).astype(BF16)
        if i == 0:
            rtok[0] = total
            return
        pout[i] = total
        send(pout.at[i], rtok.at[hops[i]], rzs.at[i], rzr.at[i], zdev(-hops[i]))

    rows = att.shape[1]
    top_half, low_half = pl.ds(0, rows // 2), pl.ds(rows // 2, rows // 2)

    def heads_ring(part):
        if part == 0:
            send(att.at[0], att.at[1], ts.at[0], tr.at[0], xdev(1))
            send(att.at[0], att.at[3], ts.at[1], tr.at[1], xdev(3))
            return
        drain(att.at[1], tr.at[0])
        send(att.at[1, top_half], att.at[2, top_half], tfs.at[0], tfr.at[0], xdev(1))
        drain(att.at[3], tr.at[1])
        send(att.at[3, low_half], att.at[2, low_half], tfs.at[1], tfr.at[1], xdev(3))

    steps = {
        "Z": plane_out, "O": ring_own, "F": ring_on, "I": ring_in, "H": hidden,
        "A": act_on, "D": down, "B": plane_back, "T": heads_ring,
    }
    for step in MIDDLE if nz == 8 else plain_order(messages, far, two, nz):
        steps[step[0]](int(step[1:]))
    for step in TAIL if nz == 8 else ("T0", f"D{len(chunks) - 1}", f"B{nz - 2}", f"B{nz - 1}", "T1"):
        steps[step[0]](int(step[1:]))
    local[3].wait()
    chunk = rows // 4
    hw = att.shape[2]

    def project(c, carry):
        where = pl.ds(pl.multiple_of(c * chunk, chunk), chunk)
        total = jnp.zeros((chunk, ow.shape[1]), F32)
        for q in range(NTP):
            total += jnp.dot(att[q, where, :], ow[quarter(-q, hw), :], preferred_element_type=F32)
        mix[where, :] = total.astype(BF16)
        return carry

    for i in range(1, nz):
        drain(rtok.at[hops[i]], rzr.at[i])

    def combined(t):
        where = pl.ds(pl.multiple_of(t * per_group, per_group), per_group)
        found = []
        for g in range(GROUPS):
            total = jnp.zeros((per_group, fq), F32)
            for p in range(planes):
                d = lax.rem(g * planes + p + nz - z, nz)
                total += rtok[d, where, :].astype(F32)
            found.append(total.astype(BF16))
        return jnp.concatenate(found, axis=0)

    for q in (2, 1, 3):
        fin_out[q] = combined(column(q))
        send(fin_out.at[q], fin.at[q], es.at[q], er.at[q], xdev(q))
    drain(att.at[2, top_half], tfr.at[0])
    drain(att.at[2, low_half], tfr.at[1])
    lax.fori_loop(0, 4, project, 0)
    mixed = pltpu.make_async_copy(mix, mix_hbm, loc.at[15])
    mixed.start()
    own = combined(x)
    turned = order[:, pl.ds(pl.multiple_of(x * block_rows, block_rows), block_rows)]
    rows, cols = iota((block_rows, block_rows), 0), iota((block_rows, block_rows), 1)
    turned = dot_nt(one_hot(rows == cols), turned.astype(BF16)).astype(jnp.int32)
    spread = one_hot(cols == turned[:, 0:1])
    moe[:, quarter(0, fq)] = jnp.dot(spread, own, preferred_element_type=F32).astype(BF16)
    for q in (1, 3, 2):
        drain(fin.at[q], er.at[q])
        placed = jnp.dot(spread, fin[q], preferred_element_type=F32).astype(BF16)
        moe[:, quarter(-q, fq)] = placed

    mixed.wait()
    for k, (i, q) in enumerate(messages):
        drain(cin_e.at[near.index(i)] if i in near else cin.at[i, q // 2], zs.at[k])
    for i in range(nz):
        drain(arr.at[0, i, rest], ys.at[i])
        if i in near or i in two:
            drain(others(i), yes.at[i])
        drain(back.at[i, rest], rys.at[i])
        if i > 0:
            drain(min_.at[i], ms.at[i])
            drain(pout.at[i], rzs.at[i])
        if i in near:
            continue
        for way in range(2):
            drain(arr.at[0, i], xs.at[i, way])
            if i not in two:
                drain(arr.at[0, i, low], fs.at[i, way])
    for c in range(len(chunks)):
        span, _ = span_of(c)
        for way in range(2):
            drain(act.at[0, span], acs.at[c, way])
            drain(act.at[0, span, 0], afs.at[c, way])
    for way in range(2):
        drain(att.at[0], ts.at[way])
        drain(att.at[0, top_half], tfs.at[way])
        drain(kvt.at[way, :, pl.ds(0, WINDOW)], hs.at[way])
    for q in range(1, NTP):
        drain(wq.at[q], ws.at[q])
        drain(fin_out.at[q], es.at[q])


def per_device(
    q_heads,
    k_heads,
    v_heads,
    sink_logits,
    out_weight,
    tokens_b,
    moe_gain,
    router_group,
    router_expert,
    route_expert,
    expert_gate,
    expert_up,
    expert_down,
):
    nyc = min(PLANE, lax.axis_size("ep"))
    nz = lax.axis_size("ep") // nyc
    tokens, width = tokens_b.shape
    fq = width // NTP
    hq = expert_gate.shape[2]
    sixteen = NTP * CAP
    span = q_heads.shape[0]
    vmem = pl.BlockSpec(memory_space=pltpu.VMEM)
    smem = pl.BlockSpec(memory_space=pltpu.SMEM)
    anywhere = pl.BlockSpec(memory_space=pl.ANY)
    dma = pltpu.SemaphoreType.DMA
    chunks = len(CHUNKS if nz == 8 else plain_chunks(nz))
    near = len(near_positions(nz))
    slot = (nz, nyc, 2, sixteen, fq)
    group_rows = tokens // GROUPS
    return pl.pallas_call(
        functools.partial(step_kernel, nz, nyc),
        out_shape=(
            jax.ShapeDtypeStruct((span, out_weight.shape[1]), BF16),
            jax.ShapeDtypeStruct((tokens // NTP, width), BF16),
        ),
        in_specs=[anywhere] * 3 + [smem] + [anywhere] * 9,
        out_specs=(anywhere, vmem),
        scratch_shapes=[
            pltpu.VMEM((1, width), F32),
            pltpu.VMEM((router_group.shape[1], width), BF16),
            pltpu.VMEM(router_expert.shape, BF16),
            pltpu.VMEM((2, tokens), jnp.int32),
            pltpu.VMEM((span, out_weight.shape[1]), BF16),
            pltpu.VMEM(tokens_b.shape, BF16),
            pltpu.VMEM(tokens_b.shape, BF16),
            pltpu.VMEM(tokens_b.shape, BF16),
            pltpu.VMEM((GROUPS, 16, group_rows), F32),
            pltpu.VMEM((8, tokens), F32),
            pltpu.VMEM((nz, 2, group_rows, fq), BF16),
            pltpu.VMEM((near, group_rows, width), BF16),
            pltpu.VMEM((nz, 16, group_rows), F32),
            pltpu.VMEM((nz, group_rows, 16), F32),
            pltpu.VMEM((len(slot_entries(nz)), *slot[1:]), BF16),
            pltpu.VMEM((NTP, *slot), BF16),
            pltpu.VMEM(expert_gate.shape, BF16),
            pltpu.VMEM(expert_up.shape, BF16),
            pltpu.VMEM((NTP, 2, hq, fq), BF16),
            pltpu.VMEM((NTP, nz, 2, nyc * sixteen, hq), BF16),
            pltpu.VMEM(slot, BF16),
            pltpu.VMEM(slot, BF16),
            pltpu.VMEM((nz, group_rows, fq), BF16),
            pltpu.VMEM((nz, group_rows, fq), BF16),
            pltpu.VMEM((NTP, *q_heads.shape), BF16),
            pltpu.VMEM(out_weight.shape, BF16),
            pltpu.VMEM((NTP, tokens // NTP, fq), BF16),
            pltpu.VMEM((NTP, tokens // NTP, fq), BF16),
            pltpu.VMEM(q_heads.shape, BF16),
            pltpu.VMEM((2, HD, span + WINDOW), BF16),
            pltpu.VMEM((2, q_heads.shape[1] // HD, q_heads.shape[1], span + WINDOW), BF16),
            dma((2 * nz,)), dma((2 * nz,)), dma((nz,)), dma((nz,)),
            dma((nz,)), dma((nz,)), dma((nz,)), dma((nz,)),
            dma((nz, 2)), dma((nz, 2)), dma((nz, 2)), dma((nz, 2)),
            dma((chunks, 2)), dma((chunks, 2)), dma((chunks, 2)), dma((chunks, 2)),
            dma((NTP,)), dma((NTP,)),
            dma((nz,)), dma((nz,)), dma((nz,)), dma((nz,)),
            dma((2,)), dma((2,)), dma((2,)), dma((2,)),
            dma((NTP,)), dma((NTP,)), dma((2,)), dma((2,)), dma((16,)),
        ],
        compiler_params=pltpu.CompilerParams(
            collective_id=0, has_side_effects=True, vmem_limit_bytes=62 * 2**20
        ),
        name="step",
    )(
        q_heads,
        k_heads.T,
        v_heads.T,
        sink_logits,
        out_weight,
        tokens_b,
        moe_gain.reshape(1, width),
        router_group.T,
        router_expert,
        route_expert.T,
        expert_gate,
        expert_up,
        expert_down,
    )


def solution(mesh):
    in_specs = (
        P("ep", "tp"),
        P("ep", "tp"),
        P("ep", "tp"),
        P("tp"),
        P(None, "tp"),
        P("ep", None),
        P(),
        P(),
        P(),
        P("ep", None),
        P("ep", None, "tp"),
        P("ep", None, "tp"),
        P("ep", "tp", None),
    )
    out_specs = (P("ep", "tp"), P(("ep", "tp"), None))
    return jax.shard_map(
        per_device, mesh=mesh, in_specs=in_specs, out_specs=out_specs, check_vma=False
    )
```

time: 166 us -> 140 us (0.84)
  Pallas kernels: 162 us -> 136 us
    pallas_call x1, Pallas kernels: 162 us -> 136 us  [per_device(): pl.pallas_call(functools.partial(step_kernel, nz, nyc), out_shape=(jax.Sh...]
where the time goes in v3:
time: 140 us
  Pallas kernels  136 us (97%)
  local copies, waits for them, and re-layouts  3.12 us (2%)
    pallas_call x1, Pallas kernels, per_device(): pl.pallas_call(functools.partial(step_kernel, nz, nyc), out_shape=(jax.Sh...  136 us
    unnamed x4, local copies, waits for them, and re-layouts  3.12 us

profile of v3, /device:TPU:1, one launch (start us, length us, event | category | flops | bytes accessed | tf_op | source)
XLA Modules:
  0.0 139.5 jit_solution(10959844160989549018)
XLA Ops:
  0.6 135.8 %step.1 = (bf16[1024,512]{1,0:T(8,128)(2,1)}, bf16[128,2048]{1,0:T(8,128)(2,1)}) custom-call(bf16[1024,256]{1,0:T(8,128)(2,1)} %q_hbm.1, bf16[64,1024]{1,0:T(8,128)(2,1)} %bitcast.5, bf16[64,1024]{1,0:T(8,128)(2,1)} %bitcast.6, f32[4]{0:T(128)} %sink.1, bf16[1024,512]{1,0:T(8,128)(2,1)} %ow_hbm.1, bf16[512,2048]{1,0:T(8,128)(2,1)} %tok_hbm.1, ...), custom_call_target="tpu_custom_call" | custom-call | tf_op jit(solution)/shard_map/step/pallas_call | solution.py:579
  136.4 0.0 copy-start
  136.4 2.3 %copy.17 = bf16[1024,512]{1,0:T(8,128)(2,1)} copy(bf16[1024,512]{1,0:T(8,128)(2,1)} %get-tuple-element.4) | data formatting | bytes 2097152
  138.7 0.0 copy-done
  138.7 0.8 copy.18
Async XLA Ops:
  136.4 2.3 %copy-start = (bf16[128,2048]{1,0:T(8,128)(2,1)S(1)}, bf16[128,2048]{1,0:T(8,128)(2,1)}, u32[]{:S(2)}) copy-start(bf16[128,2048]{1,0:T(8,128)(2,1)} %get-tuple-element.5) | copy-start | bytes 1572868

commit v4 on v3

--- a/solution.py
+++ b/solution.py
@@ -28,6 +28,7 @@
     "D4", "B6", "B7", "B0", "T1",
 )
 AHEAD = 2
+WIDEN = 2
 MESH = pl.DeviceIdType.MESH
 F32 = jnp.float32
 BF16 = jnp.bfloat16
@@ -277,8 +278,9 @@
         i, first_q = (0, 0) if k < 0 else messages[k]
         if i > 0:
             drain(cin_e.at[near.index(i)] if i in near else cin.at[i, first_q // 2], zr.at[k])
-            if k + AHEAD < len(messages):
-                plane_send(k + AHEAD)
+            for following in range(k + AHEAD + (k > WIDEN), k + AHEAD + 1 + (k >= WIDEN)):
+                if following < len(messages):
+                    plane_send(following)
             if first_q == 0:
                 drain(min_.at[i], mr.at[i])
         given = min_[i]

time: 140 us -> 137 us (0.979)
  Pallas kernels: 136 us -> 133 us
    pallas_call x1, Pallas kernels: 136 us -> 133 us  [per_device(): pl.pallas_call(functools.partial(step_kernel, nz, nyc), out_shape=(jax.Sh...]
where the time goes in v4:
time: 137 us
  Pallas kernels  133 us (97%)
  local copies, waits for them, and re-layouts  3.12 us (2%)
    pallas_call x1, Pallas kernels, per_device(): pl.pallas_call(functools.partial(step_kernel, nz, nyc), out_shape=(jax.Sh...  133 us
    unnamed x4, local copies, waits for them, and re-layouts  3.12 us

profile of v4, /device:TPU:1, one launch (start us, length us, event | category | flops | bytes accessed | tf_op | source)
XLA Modules:
  0.0 137.2 jit_solution(15670837559745039877)
XLA Ops:
  0.6 133.4 %step.1 = (bf16[1024,512]{1,0:T(8,128)(2,1)}, bf16[128,2048]{1,0:T(8,128)(2,1)}) custom-call(bf16[1024,256]{1,0:T(8,128)(2,1)} %q_hbm.1, bf16[64,1024]{1,0:T(8,128)(2,1)} %bitcast.5, bf16[64,1024]{1,0:T(8,128)(2,1)} %bitcast.6, f32[4]{0:T(128)} %sink.1, bf16[1024,512]{1,0:T(8,128)(2,1)} %ow_hbm.1, bf16[512,2048]{1,0:T(8,128)(2,1)} %tok_hbm.1, ...), custom_call_target="tpu_custom_call" | custom-call | tf_op jit(solution)/shard_map/step/pallas_call | solution.py:581
  134.0 0.0 copy-start
  134.0 2.3 %copy.17 = bf16[1024,512]{1,0:T(8,128)(2,1)} copy(bf16[1024,512]{1,0:T(8,128)(2,1)} %get-tuple-element.4) | data formatting | bytes 2097152
  136.4 0.0 copy-done
  136.4 0.8 copy.18
Async XLA Ops:
  134.0 2.3 %copy-start = (bf16[128,2048]{1,0:T(8,128)(2,1)S(1)}, bf16[128,2048]{1,0:T(8,128)(2,1)}, u32[]{:S(2)}) copy-start(bf16[128,2048]{1,0:T(8,128)(2,1)} %get-tuple-element.5) | copy-start | bytes 1572868
